TPU v7x, 32 devices: a whole 2x2x4 slice. The times are simulated.
32 devices in a mesh: ep: 8 (over z, x), tp: 4 (over y, core).
Axes of the slice: x: 2, y: 2, z: 4, core: 2. Of those that a mesh axis runs over, the one named last changes fastest.
Arguments:
- x_attend: bfloat16 [4096, 2048], P('ep'), may hold values from -6 to 6
- attend_gain: float32 [2048], replicated, may hold values from 0.1 to 1.9
- w_query: bfloat16 [2048, 1024], P(None, 'tp'), may hold values from -0.125 to 0.125
- w_key: bfloat16 [2048, 512], P(None, 'tp'), may hold values from -0.125 to 0.125
- w_value: bfloat16 [2048, 512], P(None, 'tp'), may hold values from -0.125 to 0.125
- query_gain: float32 [64], replicated, may hold values from 0.1 to 1.9
- key_gain: float32 [64], replicated, may hold values from 0.1 to 1.9
- sink_logit: float32 [16], P('tp'), may hold values from 4 to 8
- w_output: bfloat16 [1024, 2048], P('tp'), may hold values from -1.5 to 1.5
- x_experts: bfloat16 [3072, 2048], P('ep'), may hold values from -6 to 6
- expert_gain: float32 [2048], replicated, may hold values from 0.1 to 1.9
- routes: int32 [3072, 2], P('ep'), may hold values from 0 to 7, all different within a row; in each aligned block of 384 rows (0 to 383, 384 to 767, ...) at most 144 rows name the same one
- group_prob: float32 [3072], P('ep'), may hold values from 0.3 to 1
- expert_prob: float32 [3072, 2], P('ep'), may hold values from 0.05 to 1
- w_gate: bfloat16 [8, 2048, 1024], P('ep', None, 'tp'), may hold values from -0.125 to 0.125
- w_up: bfloat16 [8, 2048, 1024], P('ep', None, 'tp'), may hold values from -0.125 to 0.125
- w_down: bfloat16 [8, 1024, 2048], P('ep', 'tp'), may hold values from -0.1875 to 0.1875
Outputs:
- attend_out: bfloat16 [4096, 2048], P(('ep', 'tp'))
- expert_out: bfloat16 [3072, 2048], P('ep', 'tp')
Inputs may be any that keep to these rules, and one draw needn't show every extreme that they name: `routes`: each row names 2 different experts. Among the rows of one device no expert is named more than 144 times, and in every draw some expert is named exactly 144 times by one device's rows.
All inputs are finite; a program needn't handle non-finite values.
Results may differ from a plain program's by a relative error of at most 0.012.
Values may be sent and summed in bfloat16 or wider, within the bound.
A program may use at most 64 MiB of HBM per device.

v0:
```python
import functools

import jax
import jax.numpy as jnp
from jax import lax
from jax.experimental import pallas as pl
from jax.experimental.pallas import tpu as pltpu
from jax.sharding import PartitionSpec as P

HEAD_DIM = 64
WINDOW = 128
GRID_W = 64
MESH = pl.DeviceIdType.MESH


epsilon = 1e-06
rope_base = 10000.0


def extended(x, sides, width):
    for axis, dim in sides:
        peers, length = (lax.axis_size(axis), x.shape[dim])
        up = [(i, (i + 1) % peers) for i in range(peers - 1)]
        down = [(j, i) for i, j in up]
        last = lax.slice_in_dim(x, length - width, length, axis=dim)
        initial = lax.slice_in_dim(x, 0, width, axis=dim)
        before = lax.ppermute(last, axis, up)
        after = lax.ppermute(initial, axis, down)
        x = jnp.concatenate([before, x, after], axis=dim)
    return x


def rms_scale(inputs, gain):
    values_f = inputs.astype(jnp.float32)
    scaled = values_f * lax.rsqrt(jnp.mean(values_f * values_f, axis=-1, keepdims=True) + epsilon)
    return (scaled * gain).astype(jnp.bfloat16)


def rope_tables(positions):
    grid_rows = (positions // GRID_W).astype(jnp.float32)
    grid_cols = (positions % GRID_W).astype(jnp.float32)
    half_dim = HEAD_DIM // 2
    inverse = rope_base ** (-jnp.arange(0, half_dim, 2, dtype=jnp.float32) / half_dim)
    angles = jnp.concatenate([grid_rows[:, None] * inverse, grid_cols[:, None] * inverse], axis=-1)
    return (jnp.cos(angles), jnp.sin(angles))


def head_norm_rope(projected, gain, cosine, sine_tab):
    scaled = (
        projected
        * lax.rsqrt(jnp.mean(projected * projected, axis=-1, keepdims=True) + epsilon)
        * gain
    )
    first_half, second_half = jnp.split(scaled, 2, axis=-1)
    cos_b = cosine[:, None, :]
    sin_b = sine_tab[:, None, :]
    turned = jnp.concatenate(
        [first_half * cos_b - second_half * sin_b, second_half * cos_b + first_half * sin_b],
        axis=-1,
    )
    return turned.astype(jnp.bfloat16)


def flip(a, b, count):
    total, bit = 0, 1
    while bit < count:
        total = total + lax.rem(a // bit + b // bit, 2) * bit
        bit *= 2
    return total


def turn(p, count):
    return p // 2 + lax.rem(p, 2) * (count // 2)


def exchange_kernel(
    n_ep,
    pick_ref,
    normed_ref,
    gate_ref,
    up_ref,
    down_ref,
    mix_ref,
    attn_ref,
    out_ref,
    attn_out_ref,
    send_own,
    send_other,
    rows_buf,
    part_out,
    part_keep,
    part_in,
    y_out,
    y_own,
    y_in,
    final,
    back,
    total,
    attn_in,
    attn_y_out,
    attn_y_in,
    d_send, d_recv,
    e_send, e_recv,
    p_send, p_recv,
    y_send, y_recv,
    r_send, r_recv,
    c_send, c_recv,
    s_send, s_recv,
    f_send, f_recv,
    a_send, a_recv,
):
    me = lax.axis_index("ep")
    lane = lax.axis_index("tp")
    core = lax.rem(lane, 2)
    side = lane // 2
    other_core, other_side = 1 - core, 1 - side
    partner = 2 * side + other_core
    across = 2 * other_side + core
    capacity, width = send_own.shape[1:]
    half = n_ep // 2

    barrier = pltpu.get_barrier_semaphore()

    def greet(k, carry):
        pl.semaphore_signal(
            barrier, inc=1, device_id={"ep": flip(me, k, n_ep), "tp": lane}, device_id_type=MESH
        )
        return carry

    lax.fori_loop(1, n_ep, greet, 0)
    for peer in (partner, across):
        pl.semaphore_signal(barrier, inc=1, device_id={"ep": me, "tp": peer}, device_id_type=MESH)
    pl.semaphore_wait(barrier, n_ep + 1)

    def remote(src, dst, sends, recvs, k, ep, tp):
        return pltpu.make_async_remote_copy(
            src_ref=src,
            dst_ref=dst,
            send_sem=sends.at[k],
            recv_sem=recvs.at[k],
            device_id={"ep": ep, "tp": tp},
            device_id_type=MESH,
        )

    def dispatch(k):
        dest = flip(me, k, n_ep)
        return remote(send_own.at[k], rows_buf.at[lane, k], d_send, d_recv, k, dest, lane)

    def dispatch_other(k):
        dest = flip(me, k, n_ep)
        return remote(send_other.at[k], rows_buf.at[across, k], e_send, e_recv, k, dest, lane)

    def to_partner(k):
        block = rows_buf.at[lane, k]
        return remote(block, block, p_send, p_recv, k, me, partner)

    def to_across(k):
        block = rows_buf.at[lane, k]
        return remote(block, block, y_send, y_recv, k, me, across)

    def relay(k):
        block = rows_buf.at[across, k]
        return remote(block, block, r_send, r_recv, k, me, partner)

    def sum_core(k):
        return remote(part_out.at[k], part_in.at[k], c_send, c_recv, k, me, partner)

    def sum_side(k):
        return remote(y_out.at[k], y_in.at[k], s_send, s_recv, k, me, across)

    def give_back(k):
        return remote(final.at[k], back.at[k], f_send, f_recv, k, flip(me, k, n_ep), lane)

    def attn_core(s):
        return remote(
            attn_ref.at[2 * s + other_core], attn_in.at[s], a_send, a_recv, s, me, partner
        )

    def attn_side():
        return remote(attn_y_out, attn_y_in, a_send, a_recv, 2, me, across)

    def gathered(k, quarter):
        start = pl.multiple_of(quarter * width, width)
        rows = jnp.dot(
            pick_ref[flip(me, k, n_ep)],
            normed_ref[:, pl.ds(start, width)],
            preferred_element_type=jnp.float32,
        )
        return rows.astype(jnp.bfloat16)

    def start_dispatch(p, carry):
        k = turn(p, n_ep)
        send_own[k] = gathered(k, lane)
        dispatch(k).start()

        @pl.when(k < half)
        def _():
            send_other[k] = gathered(k, across)
            dispatch_other(k).start()

        return carry

    lax.fori_loop(1, n_ep, start_dispatch, 0)
    rows_buf[lane, 0] = gathered(0, lane)
    rows_buf[across, 0] = gathered(0, across)
    attn_core(0).start()
    attn_core(1).start()
    total[...] = jnp.zeros_like(total)

    def step(t, carry):
        @pl.when(t < n_ep)
        def _():
            k0 = turn(t, n_ep)

            @pl.when(k0 > 0)
            def _():
                dispatch(k0).wait_recv()

            to_partner(k0).start()

            @pl.when(k0 >= half)
            def _():
                to_across(k0).start()

            @pl.when((k0 > 0) & (k0 < half))
            def _():
                dispatch_other(k0).wait_recv()

            @pl.when(k0 < half)
            def _():
                relay(k0).start()

        p5 = t - 4

        @pl.when((p5 >= 0) & (p5 < n_ep))
        def _():
            k5 = turn(p5, n_ep)
            sum_core(k5).wait_recv()
            y_out[k5] = (
                part_keep[k5, other_side].astype(jnp.float32)
                + part_in[k5, other_side].astype(jnp.float32)
            ).astype(jnp.bfloat16)
            sum_side(k5).start()
            y_own[k5] = part_keep[k5, side].astype(jnp.float32) + part_in[k5, side].astype(
                jnp.float32
            )

        p1 = t - 2

        @pl.when((p1 >= 0) & (p1 < n_ep))
        def _():
            k1 = turn(p1, n_ep)

            @pl.when(k1 >= half)
            def _():
                to_across(k1).wait_recv()
                relay(k1).start()

        p2 = t - 3

        @pl.when((p2 >= 0) & (p2 < n_ep))
        def _():
            k2 = turn(p2, n_ep)
            to_partner(k2).wait_recv()
            relay(k2).wait_recv()
            gate = jnp.zeros((capacity, gate_ref.shape[1]), jnp.float32)
            up = gate
            for q in range(4):
                rows = rows_buf[q, k2]
                span = slice(q * width, (q + 1) * width)
                gate += jnp.dot(rows, gate_ref[span, :], preferred_element_type=jnp.float32)
                up += jnp.dot(rows, up_ref[span, :], preferred_element_type=jnp.float32)
            hidden = (gate / (1.0 + jnp.exp(-gate)) * up).astype(jnp.bfloat16)
            for s in range(2):
                for c, target in ((other_core, part_out), (core, part_keep)):
                    start = pl.multiple_of((2 * s + c) * width, width)
                    target[k2, s] = jnp.dot(
                        hidden, down_ref[:, pl.ds(start, width)], preferred_element_type=jnp.float32
                    ).astype(jnp.bfloat16)
            sum_core(k2).start()

        p6 = t - 6

        @pl.when((p6 >= 0) & (p6 < n_ep))
        def _():
            k6 = turn(p6, n_ep)
            sum_side(k6).wait_recv()
            final[k6] = (y_own[k6] + y_in[k6].astype(jnp.float32)).astype(jnp.bfloat16)

            @pl.when(k6 > 0)
            def _():
                give_back(k6).start()

            @pl.when(k6 == 0)
            def _():
                total[...] += jnp.dot(mix_ref[me], final[0], preferred_element_type=jnp.float32)

        p7 = t - 9

        @pl.when((p7 > 0) & (p7 < n_ep))
        def _():
            k7 = turn(p7, n_ep)
            give_back(k7).wait_recv()
            total[...] += jnp.dot(
                mix_ref[flip(me, k7, n_ep)], back[k7], preferred_element_type=jnp.float32
            )

        @pl.when(t == 0)
        def _():
            attn_core(0).wait_recv()
            attn_core(1).wait_recv()
            attn_y_out[...] = (
                attn_ref[2 * other_side + core].astype(jnp.float32)
                + attn_in[other_side].astype(jnp.float32)
            ).astype(jnp.bfloat16)
            attn_side().start()

        return carry

    lax.fori_loop(0, n_ep + 9, step, 0)
    attn_side().wait_recv()
    attn_out_ref[...] = (
        attn_ref[2 * side + core].astype(jnp.float32)
        + attn_in[side].astype(jnp.float32)
        + attn_y_in[...].astype(jnp.float32)
    ).astype(jnp.bfloat16)
    out_ref[...] = total[...].astype(jnp.bfloat16)

    def drain(k, carry):
        @pl.when(k > 0)
        def _():
            dispatch(k).wait_send()
            give_back(k).wait_send()

        to_partner(k).wait_send()
        @pl.when(k >= half)
        def _():
            to_across(k).wait_send()

        @pl.when((k > 0) & (k < half))
        def _():
            dispatch_other(k).wait_send()

        relay(k).wait_send()
        sum_core(k).wait_send()
        sum_side(k).wait_send()
        return carry

    lax.fori_loop(0, n_ep, drain, 0)
    attn_core(0).wait_send()
    attn_core(1).wait_send()
    attn_side().wait_send()


def per_device(
    x_attend,
    attend_gain,
    w_query,
    w_key,
    w_value,
    query_gain,
    key_gain,
    sink_logit,
    w_output,
    x_experts,
    expert_gain,
    routes,
    group_prob,
    expert_prob,
    w_gate,
    w_up,
    w_down,
):
    tok_rows = x_attend.shape[0]
    model_width = x_attend.shape[1]
    heads_local = sink_logit.shape[0]
    kv_local = w_key.shape[1] // HEAD_DIM
    group = heads_local // kv_local
    offset = lax.axis_index("ep") * tok_rows
    positions = offset + jnp.arange(tok_rows, dtype=jnp.int32)
    cosine, sine_tab = rope_tables(positions)
    normed = rms_scale(x_attend, attend_gain)
    queries = head_norm_rope(
        jnp.dot(normed, w_query, preferred_element_type=jnp.float32).reshape(
            tok_rows, heads_local, HEAD_DIM
        ),
        query_gain,
        cosine,
        sine_tab,
    )
    key_rows = head_norm_rope(
        jnp.dot(normed, w_key, preferred_element_type=jnp.float32).reshape(
            tok_rows, kv_local, HEAD_DIM
        ),
        key_gain,
        cosine,
        sine_tab,
    )
    values = jnp.dot(normed, w_value, preferred_element_type=jnp.float32).astype(jnp.bfloat16)
    stacked = jnp.stack([key_rows.reshape(tok_rows, kv_local * HEAD_DIM), values], axis=0)
    padded = extended(stacked, (("ep", 1),), WINDOW)
    span_keys = padded[0].reshape(tok_rows + 2 * WINDOW, kv_local, HEAD_DIM)
    span_values = padded[1].reshape(tok_rows + 2 * WINDOW, kv_local, HEAD_DIM)
    scores = jnp.einsum(
        "qhgd,khd->hgqk",
        queries.reshape(tok_rows, kv_local, group, HEAD_DIM),
        span_keys,
        preferred_element_type=jnp.float32,
    ) * HEAD_DIM ** (-0.5)
    key_pos = offset - WINDOW + jnp.arange(tok_rows + 2 * WINDOW, dtype=jnp.int32)
    total_len = tok_rows * lax.axis_size("ep")
    in_window = (
        (jnp.abs(positions[:, None] - key_pos[None, :]) <= WINDOW)
        & (key_pos[None, :] >= 0)
        & (key_pos[None, :] < total_len)
    )
    scores = jnp.where(in_window[None, None], scores, -1e30)
    sink_col = sink_logit.reshape(kv_local, group)[:, :, None]
    peak = jnp.maximum(jnp.max(scores, axis=-1), sink_col)[..., None]
    weights = jnp.exp(scores - peak)
    denominator = jnp.sum(weights, axis=-1, keepdims=True) + jnp.exp(sink_col[..., None] - peak)
    probs = (weights / denominator).astype(jnp.bfloat16)
    attended = jnp.einsum("hgqk,khd->qhgd", probs, span_values, preferred_element_type=jnp.float32)
    attended = attended.astype(jnp.bfloat16).reshape(tok_rows, heads_local * HEAD_DIM)
    tp_count = lax.axis_size("tp")
    attn_part = (
        jnp.dot(attended, w_output, preferred_element_type=jnp.float32)
        .astype(jnp.bfloat16)
        .reshape(tp_count, tok_rows // tp_count, model_width)
    )
    moe_rows = x_experts.shape[0]
    top_count = routes.shape[1]
    n_ep = lax.axis_size("ep")
    capacity = max(2, (3 * moe_rows * top_count + 2 * n_ep - 1) // (2 * n_ep))
    moe_normed = rms_scale(x_experts, expert_gain)
    col_width = model_width // tp_count
    route_weight = group_prob[:, None] * expert_prob / jnp.sum(expert_prob, axis=1, keepdims=True)
    names = jnp.arange(n_ep, dtype=jnp.int32)
    chosen = routes[:, :, None] == names[None, None, :]
    named = jnp.any(chosen, axis=1)
    token = jnp.arange(moe_rows, dtype=jnp.int32)
    earlier = (token[None, :] < token[:, None]).astype(jnp.bfloat16)
    rank = jnp.dot(earlier, named.astype(jnp.bfloat16), preferred_element_type=jnp.float32)
    rank = jnp.where(named, rank.astype(jnp.int32), -1)
    share = jnp.sum(jnp.where(chosen, route_weight[:, :, None], 0.0), axis=1)
    slots = jnp.arange(capacity, dtype=jnp.int32)
    pick = (rank.T[:, None, :] == slots[None, :, None]).astype(jnp.bfloat16)
    mix = jnp.where(
        rank.T[:, :, None] == slots[None, None, :], share.T[:, :, None], 0.0
    ).astype(jnp.bfloat16)
    hidden_cols = w_gate.shape[2]
    slice_rows = tok_rows // tp_count
    bf16, f32 = jnp.bfloat16, jnp.float32
    vmem = pl.BlockSpec(memory_space=pltpu.VMEM)
    dma = pltpu.SemaphoreType.DMA
    expert_out, attend_out = pl.pallas_call(
        functools.partial(exchange_kernel, n_ep),
        out_shape=(
            jax.ShapeDtypeStruct((moe_rows, col_width), bf16),
            jax.ShapeDtypeStruct((slice_rows, model_width), bf16),
        ),
        in_specs=[vmem] * 7,
        out_specs=(vmem, vmem),
        scratch_shapes=[
            pltpu.VMEM((n_ep, capacity, col_width), bf16),
            pltpu.VMEM((n_ep // 2, capacity, col_width), bf16),
            pltpu.VMEM((tp_count, n_ep, capacity, col_width), bf16),
            pltpu.VMEM((n_ep, 2, capacity, col_width), bf16),
            pltpu.VMEM((n_ep, 2, capacity, col_width), bf16),
            pltpu.VMEM((n_ep, 2, capacity, col_width), bf16),
            pltpu.VMEM((n_ep, capacity, col_width), bf16),
            pltpu.VMEM((n_ep, capacity, col_width), f32),
            pltpu.VMEM((n_ep, capacity, col_width), bf16),
            pltpu.VMEM((n_ep, capacity, col_width), bf16),
            pltpu.VMEM((n_ep, capacity, col_width), bf16),
            pltpu.VMEM((moe_rows, col_width), f32),
            pltpu.VMEM((2, slice_rows, model_width), bf16),
            pltpu.VMEM((slice_rows, model_width), bf16),
            pltpu.VMEM((slice_rows, model_width), bf16),
        ]
        + [dma((n_ep,))] * 16
        + [dma((3,))] * 2,
        compiler_params=pltpu.CompilerParams(
            collective_id=0, has_side_effects=True, vmem_limit_bytes=60 * 1024 * 1024
        ),
    )(pick, moe_normed, w_gate[0], w_up[0], w_down[0], mix, attn_part)
    return (attend_out, expert_out)


def solution(mesh):
    placed = (
        P("ep", None),
        P(),
        P(None, "tp"),
        P(None, "tp"),
        P(None, "tp"),
        P(),
        P(),
        P("tp"),
        P("tp", None),
        P("ep", None),
        P(),
        P("ep", None),
        P("ep"),
        P("ep", None),
        P("ep", None, "tp"),
        P("ep", None, "tp"),
        P("ep", "tp", None),
    )
    return jax.shard_map(
        per_device,
        mesh=mesh,
        in_specs=placed,
        out_specs=(P(("ep", "tp"), None), P("ep", "tp")),
        check_vma=False,
    )
```

profile of v0, /device:TPU:0, one launch (start us, length us, event | category | flops | bytes accessed | tf_op | source)
XLA Modules:
  0.0 117.0 jit_solution(10100863075038250670)
XLA Ops:
  0.6 0.0 copy-start
  0.7 0.0 copy-start.10
  0.7 2.2 %fusion.2 = f32[512]{0:T(512)S(1)} fusion(bf16[512,2048]{1,0:T(8,128)(2,1)} %param.17), kind=kLoop, calls=%fused_computation.7 | loop fusion | flops 3145216 | bytes 2099200 | tf_op jit(solution)/shard_map/reduce_sum | solution.py:35
  2.9 0.0 copy-start.3
  2.9 0.0 copy-start.11
  2.9 0.0 copy-start.9
  2.9 2.7 %multiply_reduce_fusion.1 = (f32[512,2]{0,1:T(2,128)S(1)}, f32[512,128]{0,1:T(8,128)S(1)}) fusion(bf16[2048,128]{1,0:T(8,128)(2,1)} %param.20, bf16[512,2048]{1,0:T(8,128)(2,1)} %param.17, f32[2048]{0:T(1024)} %param.18, f32[512]{0:T(512)S(1)} %add_rsqrt_fusion.2), kind=kOutput, calls=%fused_computation.40 | convolution fusion | flops 272759808 | bytes 2897920 | tf_op jit(solution)/shard_map/dot_general | solution.py:392
  5.7 0.1 broadcast_multiply_fusion.1
  5.7 0.2 fusion.20
  6.0 0.0 copy-done.10
  6.0 0.1 multiply_multiply_fusion.1
  6.2 0.1 copy.31
  6.3 0.0 copy-done.3
  6.3 0.0 copy-done.11
  6.3 1.8 %fusion.13 = bf16[1,512,128]{2,1,0:T(8,128)(2,1)S(1)} fusion(bf16[2048,128]{1,0:T(8,128)(2,1)} %param.21, bf16[512,2048]{1,0:T(8,128)(2,1)S(1)} %copy-done.3, f32[2048]{0:T(1024)S(1)} %copy-done.11, f32[512]{0:T(512)S(1)} %add_rsqrt_fusion.2), kind=kOutput, calls=%fused_computation.26 | convolution fusion | flops 272695296 | bytes 2762752 | tf_op jit(solution)/shard_map/dot_general | solution.py:399
  8.1 0.0 copy-done.9
  8.1 0.7 pad_maximum_fusion.3
  8.8 5.5 %collective-permute-start = (bf16[2,128,128]{2,1,0:T(8,128)(2,1)}, bf16[2,128,128]{2,1,0:T(8,128)(2,1)}, u32[]{:S(2)}, u32[]{:S(2)}) collective-permute-start(bf16[2,128,128]{2,1,0:T(8,128)(2,1)} %get-tuple-element.12), channel_id=1, source_target_pairs={{0,4},{4,8},{8,12},{12,16},{16,20},{20,24},{24,28},{1,5},{5,9},{9,... | collective-permute-start | bytes 196616 | tf_op jit(solution)/shard_map/ppermute | solution.py:27
  14.3 1.5 %collective-permute-start.1 = (bf16[2,128,128]{2,1,0:T(8,128)(2,1)}, bf16[2,128,128]{2,1,0:T(8,128)(2,1)}, u32[]{:S(2)}, u32[]{:S(2)}) collective-permute-start(bf16[2,128,128]{2,1,0:T(8,128)(2,1)} %get-tuple-element.13), channel_id=1, source_target_pairs={{4,0},{8,4},{12,8},{16,12},{20,16},{24,20},{28,24},{5,1},{9,5},{13... | collective-permute-start | bytes 196616 | tf_op jit(solution)/shard_map/ppermute | solution.py:28
  15.7 0.6 fusion.22
  16.3 0.0 copy-start.4
  16.3 0.0 copy-start.5
  16.3 2.2 %multiply_reduce_fusion = (f32[512,4]{0,1:T(4,128)S(1)}, f32[512,256]{0,1:T(8,128)S(1)}) fusion(bf16[2048,256]{1,0:T(8,128)(2,1)} %param.19, bf16[512,2048]{1,0:T(8,128)(2,1)S(1)} %copy-done.3, f32[2048]{0:T(1024)} %param.18, f32[512]{0:T(512)} %copy-done.9), kind=kOutput, calls=%fused_computation.31 | convolution fusion | flops 541325312 | bytes 3688448 | tf_op jit(solution)/shard_map/dot_general | solution.py:384
  18.5 0.0 copy-start.2
  18.5 0.0 copy-start.6
  18.6 0.9 multiply_multiply_fusion
  19.4 0.1 subtract_convert_fusion
  19.5 0.0 copy-done.4
  19.6 0.1 fusion.14
  19.7 0.0 copy-done.5
  19.8 0.7 multiply_divide_fusion
  20.5 1.2 fusion.9.pick_ref
  21.6 0.0 copy-start.7
  21.6 0.0 copy-start.8
  21.6 0.0 copy-start.12
  21.6 2.3 %select_convert_fusion.mix_ref = bf16[8,384,144]{2,1,0:T(8,128)(2,1)} fusion(bf16[8,384]{1,0:T(8,128)(2,1)S(1)} %bitcast.60, s32[8,384]{1,0:T(8,128)S(1)} %fusion.14), kind=kLoop, calls=%fused_computation.15 | loop fusion | flops 884736 | bytes 903168 | tf_op jit(solution)/shard_map/convert_element_type | solution.py:450
  24.0 0.0 copy-done.2
  24.0 0.4 fusion.5
  24.4 0.0 copy-done.6
  24.4 1.6 %fusion.7.normed_ref = bf16[384,2048]{1,0:T(8,128)(2,1)} fusion(bf16[384,2048]{1,0:T(8,128)(2,1)S(1)} %copy-done.2, f32[2048]{0:T(1024)S(1)} %copy-done.6, f32[384]{0:T(512)S(1)} %add_rsqrt_fusion.3), kind=kLoop, calls=%fused_computation.14 | loop fusion | flops 3145728 | bytes 3155456 | tf_op jit(solution)/shard_map/convert_element_type | solution.py:36
  25.9 0.0 copy-done.7
  25.9 0.0 copy-done.8
  26.0 0.7 fusion.11
  26.7 0.0 copy-done.12
  26.7 0.1 max.17
  26.8 0.0 collective-permute-done
  26.8 0.0 collective-permute-done.1
  26.8 0.9 pad_maximum_fusion
  27.7 0.1 copy.33
  27.9 1.3 %fusion.1 = (f32[2,2,512]{2,1,0:T(2,128)S(1)}, f32[2,768,512,2]{2,1,3,0:T(8,128)S(1)}) fusion(pred[512,768]{0,1:T(8,128)(4,1)S(1)} %fusion.11, bf16[768,2,64,1]{0,2,3,1:T(8,128)(2,1)S(1)} %bitcast.56, bf16[512,2,2,32]{0,3,2,1:T(8,128)(2,1)S(1)} %bitcast.59, bf16[512,2,2,32]{0,3,2,1:T(8,128)(2,1)S(1)} %bitcast.58), kind=kOutput, calls=%fused_computation.6 | convolution fusion | flops 206567424 | bytes 7151616 | tf_op jit(solution)/shard_map/qhgd,khd->hgqk/dot_general | solution.py:404
  29.2 0.0 copy-start.1
  29.2 0.1 broadcast_maximum_fusion
  29.3 1.4 %fusion = f32[2,2,512]{2,1,0:T(2,128)S(1)} fusion(f32[2,768,512,2]{2,1,3,0:T(8,128)S(1)} %get-tuple-element.23, f32[2,2,512]{2,1,0:T(2,128)S(1)} %broadcast_maximum_fusion, pred[512,768]{0,1:T(8,128)(4,1)S(1)} %fusion.11), kind=kLoop, calls=%fused_computation.3 | loop fusion | flops 6289408 | bytes 6701056 | tf_op jit(solution)/shard_map/reduce_sum | solution.py:421
  30.6 1.2 %copy-done.1 = f32[2,768,512,2]{2,1,3,0:T(8,128)} copy-done((f32[2,768,512,2]{2,1,3,0:T(8,128)}, f32[2,768,512,2]{2,1,3,0:T(8,128)S(1)}, u32[]{:S(2)}) %copy-start.1) | copy-done | bytes 6291480
  31.8 0.1 exponential_add_fusion
  31.9 0.1 copy.32
  32.1 4.7 %fusion.12 = bf16[2,64,2,512]{3,1,2,0:T(8,128)(2,1)S(1)} fusion(bf16[768,2,64,1]{0,2,3,1:T(8,128)(2,1)S(1)} %bitcast.57, f32[2,768,512,2]{2,1,3,0:T(8,128)} %copy-done.1, f32[2,2,512]{2,1,0:T(2,128)S(1)} %exponential_add_fusion, f32[2,2,512]{2,1,0:T(2,128)S(1)} %broadcast_maximum_fusion, pred[512,768]{0,1:T(8,128)(4,1)S(1)} %fusion.11), kind=kOutput, calls=%fused_computation.24 | convolution fusion | flops 209321984 | bytes 7159808 | tf_op jit(solution)/shard_map/hgqk,khd->qhgd/dot_general | solution.py:423
  36.8 0.0 copy-done
  36.8 2.1 %convolution_convert_fusion = bf16[512,2048]{1,0:T(8,128)(2,1)} fusion(bf16[512,256]{0,1:T(8,128)(2,1)S(1)} %bitcast.54, bf16[256,2048]{1,0:T(8,128)(2,1)S(1)} %copy-done), kind=kOutput, calls=%fused_computation.18 | convolution fusion | flops 537919488 | bytes 3407872 | tf_op jit(solution)/shard_map/dot_general | solution.py:427
  38.9 74.5 %shard_map.176 = (bf16[384,512]{1,0:T(8,128)(2,1)}, bf16[128,2048]{1,0:T(8,128)(2,1)}) custom-call(bf16[8,144,384]{2,1,0:T(8,128)(2,1)} %fusion.9.pick_ref, bf16[384,2048]{1,0:T(8,128)(2,1)} %fusion.7.normed_ref, bf16[2048,256]{1,0:T(8,128)(2,1)} %bitcast.51, bf16[2048,256]{1,0:T(8,128)(2,1)} %bitcast.52, bf16[256,2048]{1,0:T(8,128)(2,1)} %bitcast.53, ...), custom_call_target="tpu_custom_call" | custom-call | tf_op jit(solution)/shard_map/pallas_call | solution.py:456
  113.3 1.9 %copy.40 = bf16[128,2048]{1,0:T(8,128)(2,1)} copy(bf16[128,2048]{1,0:T(8,128)(2,1)} %get-tuple-element.30) | data formatting | bytes 1048576
  115.2 1.8 %copy.41 = bf16[384,512]{1,0:T(8,128)(2,1)} copy(bf16[384,512]{1,0:T(8,128)(2,1)} %get-tuple-element.31) | data formatting | bytes 786432
  (14 shorter events, 0.2 us)
Async XLA Ops:
  0.6 36.1 %copy-start = (bf16[256,2048]{1,0:T(8,128)(2,1)S(1)}, bf16[256,2048]{1,0:T(8,128)(2,1)}, u32[]{:S(2)}) copy-start(bf16[256,2048]{1,0:T(8,128)(2,1)} %param.25) | copy-start | bytes 3145732
  0.7 5.3 %copy-start.10 = (f32[64]{0:T(128)S(1)}, f32[64]{0:T(128)}, u32[]{:S(2)}) copy-start(f32[64]{0:T(128)} %param.23) | copy-start | bytes 772
  2.9 3.4 %copy-start.3 = (bf16[512,2048]{1,0:T(8,128)(2,1)S(1)}, bf16[512,2048]{1,0:T(8,128)(2,1)}, u32[]{:S(2)}) copy-start(bf16[512,2048]{1,0:T(8,128)(2,1)} %param.17) | copy-start | bytes 6291460
  2.9 3.4 %copy-start.11 = (f32[2048]{0:T(1024)S(1)}, f32[2048]{0:T(1024)}, u32[]{:S(2)}) copy-start(f32[2048]{0:T(1024)} %param.18) | copy-start | bytes 24580
  2.9 5.2 %copy-start.9 = (f32[512]{0:T(512)}, f32[512]{0:T(512)S(1)}, u32[]{:S(2)}) copy-start(f32[512]{0:T(512)S(1)} %add_rsqrt_fusion.2) | copy-start | bytes 6148
  8.8 18.0 %collective-permute-start = (bf16[2,128,128]{2,1,0:T(8,128)(2,1)}, bf16[2,128,128]{2,1,0:T(8,128)(2,1)}, u32[]{:S(2)}, u32[]{:S(2)}) collective-permute-start(bf16[2,128,128]{2,1,0:T(8,128)(2,1)} %get-tuple-element.12), channel_id=1, source_target_pairs={{0,4},{4,8},{8,12},{12,16},{16,20},{20,24},{24,28},{1,5},{5,9},{9,... | collective-permute-start | bytes 196616 | tf_op jit(solution)/shard_map/ppermute | solution.py:27
  14.3 12.5 %collective-permute-start.1 = (bf16[2,128,128]{2,1,0:T(8,128)(2,1)}, bf16[2,128,128]{2,1,0:T(8,128)(2,1)}, u32[]{:S(2)}, u32[]{:S(2)}) collective-permute-start(bf16[2,128,128]{2,1,0:T(8,128)(2,1)} %get-tuple-element.13), channel_id=1, source_target_pairs={{4,0},{8,4},{12,8},{16,12},{20,16},{24,20},{28,24},{5,1},{9,5},{13... | collective-permute-start | bytes 196616 | tf_op jit(solution)/shard_map/ppermute | solution.py:28
  16.3 3.2 %copy-start.4 = (s32[384,2]{0,1:T(2,128)S(1)}, s32[384,2]{0,1:T(2,128)}, u32[]{:S(2)}) copy-start(s32[384,2]{0,1:T(2,128)} %param.28) | copy-start | bytes 9220
  16.3 3.4 %copy-start.5 = (f32[384,2]{0,1:T(2,128)S(1)}, f32[384,2]{0,1:T(2,128)}, u32[]{:S(2)}) copy-start(f32[384,2]{0,1:T(2,128)} %param.30) | copy-start | bytes 9220
  18.5 5.5 %copy-start.2 = (bf16[384,2048]{1,0:T(8,128)(2,1)S(1)}, bf16[384,2048]{1,0:T(8,128)(2,1)}, u32[]{:S(2)}) copy-start(bf16[384,2048]{1,0:T(8,128)(2,1)} %param.26) | copy-start | bytes 4718596
  18.5 5.8 %copy-start.6 = (f32[2048]{0:T(1024)S(1)}, f32[2048]{0:T(1024)}, u32[]{:S(2)}) copy-start(f32[2048]{0:T(1024)} %param.27) | copy-start | bytes 24580
  21.6 4.3 %copy-start.7 = (pred[768]{0:T(1024)(128)(4,1)S(1)}, pred[768]{0:T(1024)(128)(4,1)}, u32[]{:S(2)}) copy-start(pred[768]{0:T(1024)(128)(4,1)} %get-tuple-element.26) | copy-start | bytes 2308
  21.6 4.3 %copy-start.8 = (pred[768]{0:T(1024)(128)(4,1)S(1)}, pred[768]{0:T(1024)(128)(4,1)}, u32[]{:S(2)}) copy-start(pred[768]{0:T(1024)(128)(4,1)} %get-tuple-element.27) | copy-start | bytes 2308
  21.6 5.1 %copy-start.12 = (f32[4]{0:T(128)S(1)}, f32[4]{0:T(128)}, u32[]{:S(2)}) copy-start(f32[4]{0:T(128)} %param.24) | copy-start | bytes 52
  29.2 2.7 %copy-start.1 = (f32[2,768,512,2]{2,1,3,0:T(8,128)}, f32[2,768,512,2]{2,1,3,0:T(8,128)S(1)}, u32[]{:S(2)}) copy-start(f32[2,768,512,2]{2,1,3,0:T(8,128)S(1)} %get-tuple-element.23) | copy-start | bytes 18874372
where the time goes:
time: 117 us
  Pallas kernels  74.5 us (64%)
  matrix products  14.9 us (13%)
  other arithmetic  14.2 us (12%)
  starting transfers between devices  6.95 us (6%)
  local copies, waits for them, and re-layouts  5.43 us (5%)
    pallas_call x1, Pallas kernels, per_device(): pl.pallas_call(functools.partial(exchange_kernel, n_ep), out_shape=(jax.S...  74.5 us
    ppermute x1, starting transfers between devices, extended(): before = lax.ppermute(last, axis, up)  5.49 us
    unnamed x28, local copies, waits for them, and re-layouts  4.91 us
    dot_general x1, matrix products, per_device(): jnp.einsum('hgqk,khd->qhgd', probs, span_values, preferred_element_type=j...  4.7 us
    dot_general x1, matrix products, per_device(): jnp.dot(normed, w_key, preferred_element_type=jnp.float32)  2.74 us
    reduce_sum x2, other arithmetic, rms_scale(): jnp.mean(values_f * values_f, axis=-1, keepdims=True) + epsilon  2.54 us
    convert_element_type x1, other arithmetic, per_device(): mix = jnp.where(rank.T[:, :, None] == slots[None, None, :], share.T[:, :,...  2.34 us
  transfers between devices with their start and end apart: 2, of which 0 were waited for; matrix products, arithmetic and copies ran while one was open for 9% of the time, Pallas kernels for 0%

commit v1 on v0

v1 whole, which is shorter than its diff:
```python
import functools

import jax
import jax.numpy as jnp
from jax import lax
from jax.experimental import pallas as pl
from jax.experimental.pallas import tpu as pltpu
from jax.sharding import PartitionSpec as P

HEAD_DIM = 64
WINDOW = 128
GRID_W = 64
MESH = pl.DeviceIdType.MESH
EPSILON = 1e-06
LOG_BASE = 9.210340371976184
ATTN_CHUNKS = 4
bf16, f32, i32 = jnp.bfloat16, jnp.float32, jnp.int32


def flip(a, b, count):
    total, bit = 0, 1
    while bit < count:
        total = total + lax.rem(a // bit + b // bit, 2) * bit
        bit *= 2
    return total


def iota(shape, dim):
    return lax.broadcasted_iota(i32, shape, dim)


def dot(a, b):
    return jnp.dot(a, b, preferred_element_type=f32)


def dot_nt(a, b):
    return lax.dot_general(a, b, (((1,), (1,)), ((), ())), preferred_element_type=f32)


def one_zero(mask):
    return jnp.where(mask, 1.0, 0.0).astype(bf16)


def rms_inplace(ref, gain_ref, chunk):
    def body(i, carry):
        rows = pl.ds(pl.multiple_of(i * chunk, chunk), chunk)
        v = ref[rows, :].astype(f32)
        scale = lax.rsqrt(jnp.mean(v * v, axis=-1, keepdims=True) + EPSILON)
        ref[rows, :] = (v * scale * gain_ref[...]).astype(bf16)
        return carry

    lax.fori_loop(0, ref.shape[0] // chunk, body, 0)


def fused_kernel(
    n_ep,
    xa_hbm, a_gain, wq_hbm, wk_hbm, wv_hbm, q_gain, k_gain, sink, wo_hbm,
    xe_hbm, e_gain, routes_t, group_p, expert_p, wg_hbm, wu_hbm, wd_hbm,
    out_ref, attn_out_ref,
    xa, wqkv, wo, xe, wgu, wd,
    ctab, stab, q_s, kv, halo, kd, ve, att,
    attn_ref, attn_in, attn_y_out, attn_y_in,
    rank_s, rank_tn, share_tn, mix,
    send_own, send_other, rows_buf, part_out, part_keep, part_in,
    y_out, y_own, y_in, final, back, total,
    l_sem,
    d_send, d_recv, e_send, e_recv, p_send, p_recv, y_send, y_recv,
    r_send, r_recv, c_send, c_recv, s_send, s_recv, f_send, f_recv,
    a_send, a_recv, b_send, b_recv, h_send, h_recv,
):
    me = lax.axis_index("ep")
    lane = lax.axis_index("tp")
    core = lax.rem(lane, 2)
    side = lane // 2
    other_core, other_side = 1 - core, 1 - side
    partner = 2 * side + other_core
    across = 2 * other_side + core
    capacity, width = send_own.shape[1:]
    half = n_ep // 2
    tokens = xa.shape[0]
    moe_tokens = xe.shape[0]
    kv_local, ext_rows, pair = kd.shape
    q_cols = q_s.shape[1]
    hidden_cols = wd.shape[0]

    def local(i, src, dst):
        return pltpu.make_async_copy(src, dst, l_sem.at[i])

    kw = wk_hbm.shape[1]
    loads = [
        local(0, xe_hbm, xe),
        local(1, wg_hbm, wgu.at[:, 0:hidden_cols]),
        local(2, wu_hbm, wgu.at[:, hidden_cols : 2 * hidden_cols]),
        local(3, wd_hbm, wd),
        local(4, xa_hbm, xa),
        local(5, wq_hbm, wqkv.at[:, 0:q_cols]),
        local(6, wk_hbm, wqkv.at[:, q_cols : q_cols + kw]),
        local(7, wv_hbm, wqkv.at[:, q_cols + kw : q_cols + 2 * kw]),
        local(8, wo_hbm, wo),
    ]
    loads[0].start()

    barrier = pltpu.get_barrier_semaphore()

    def greet(k, carry):
        pl.semaphore_signal(
            barrier, inc=1, device_id={"ep": flip(me, k, n_ep), "tp": lane}, device_id_type=MESH
        )
        return carry

    lax.fori_loop(1, n_ep, greet, 0)
    for peer in (partner, across):
        pl.semaphore_signal(barrier, inc=1, device_id={"ep": me, "tp": peer}, device_id_type=MESH)

    def remote(src, dst, sends, recvs, k, ep, tp):
        return pltpu.make_async_remote_copy(
            src_ref=src,
            dst_ref=dst,
            send_sem=sends.at[k],
            recv_sem=recvs.at[k],
            device_id={"ep": ep, "tp": tp},
            device_id_type=MESH,
        )

    def dispatch(k):
        dest = flip(me, k, n_ep)
        return remote(send_own.at[k], rows_buf.at[lane, k], d_send, d_recv, k, dest, lane)

    def dispatch_other(k):
        dest = flip(me, k, n_ep)
        return remote(send_other.at[k], rows_buf.at[across, k], e_send, e_recv, k, dest, lane)

    def to_partner(k):
        block = rows_buf.at[lane, k]
        return remote(block, block, p_send, p_recv, k, me, partner)

    def to_across(k):
        block = rows_buf.at[lane, k]
        return remote(block, block, y_send, y_recv, k, me, across)

    def relay(k):
        block = rows_buf.at[across, k]
        return remote(block, block, r_send, r_recv, k, me, partner)

    def sum_core(k):
        return remote(part_out.at[k], part_in.at[k], c_send, c_recv, k, me, partner)

    def sum_side(k):
        return remote(y_out.at[k], y_in.at[k], s_send, s_recv, k, me, across)

    def give_back(k):
        return remote(final.at[k], back.at[k], f_send, f_recv, k, flip(me, k, n_ep), lane)

    def attn_core(s):
        return remote(
            attn_ref.at[2 * s + other_core], attn_in.at[s], a_send, a_recv, s, me, partner
        )

    chunk_rows = attn_y_out.shape[1]

    def attn_side(c):
        return remote(attn_y_out.at[c], attn_y_in.at[c], b_send, b_recv, c, me, across)

    def halo_up():
        return remote(
            kv.at[tokens - WINDOW : tokens], halo.at[0], h_send, h_recv, 0, me + 1, lane
        )

    def halo_down():
        return remote(kv.at[0:WINDOW], halo.at[1], h_send, h_recv, 1, me - 1, lane)

    def plan():
        names = iota((n_ep, moe_tokens), 0)
        named = None
        share = jnp.zeros((n_ep, moe_tokens), f32)
        top = routes_t.shape[0]
        prob_sum = expert_p[0:1, :]
        for j in range(1, top):
            prob_sum = prob_sum + expert_p[j : j + 1, :]
        for j in range(top):
            chosen = routes_t[j : j + 1, :] == names
            weight = group_p[...] * expert_p[j : j + 1, :] / prob_sum
            share = share + jnp.where(chosen, weight, 0.0)
            named = chosen if named is None else named | chosen
        before = one_zero(iota((moe_tokens, moe_tokens), 0) < iota((moe_tokens, moe_tokens), 1))
        same = one_zero(iota((moe_tokens, moe_tokens), 0) == iota((moe_tokens, moe_tokens), 1))
        rank = jnp.where(named, dot(one_zero(named), before), -1.0)
        rank_s[...] = rank
        rank_tn[...] = dot_nt(same, rank.astype(bf16))
        share_tn[...] = dot_nt(same, share.astype(bf16))

    def pick(k):
        row = rank_s[pl.ds(flip(me, k, n_ep), 1), :]
        return one_zero(row == iota((capacity, moe_tokens), 0).astype(f32))

    def gathered(chosen, quarter):
        start = pl.multiple_of(quarter * width, width)
        return dot(chosen, xe[:, pl.ds(start, width)]).astype(bf16)

    def D(k, near):
        chosen = pick(k)
        send_own[k] = gathered(chosen, lane)
        dispatch(k).start()
        if near:
            send_other[k] = gathered(chosen, across)
            dispatch_other(k).start()

    def L0():
        chosen = pick(0)
        rows_buf[lane, 0] = gathered(chosen, lane)
        to_partner(0).start()
        rows_buf[across, 0] = gathered(chosen, across)
        relay(0).start()

    def build_mix():
        columns = iota((moe_tokens, n_ep), 1)
        slots = iota((moe_tokens, capacity), 1).astype(f32)

        def body(e, carry):
            rank = jnp.sum(jnp.where(columns == e, rank_tn[...], 0.0), axis=1, keepdims=True)
            share = jnp.sum(jnp.where(columns == e, share_tn[...], 0.0), axis=1, keepdims=True)
            mix[e] = jnp.where(rank == slots, share, 0.0).astype(bf16)
            return carry

        lax.fori_loop(0, n_ep, body, 0)

    def A(k, near):
        dispatch(k).wait_recv()
        if near:
            to_partner(k).start()
            dispatch_other(k).wait_recv()
            relay(k).start()
        else:
            to_across(k).start()
            to_partner(k).start()

    def B(k):
        to_across(k).wait_recv()
        relay(k).start()

    def C(k):
        to_partner(k).wait_recv()
        relay(k).wait_recv()
        rows = jnp.concatenate([rows_buf[q, k] for q in range(4)], axis=1)
        acts = dot(rows, wgu[...])
        gate, up = acts[:, 0:hidden_cols], acts[:, hidden_cols:]
        hidden = (gate / (1.0 + jnp.exp(-gate)) * up).astype(bf16)
        for c, target in ((other_core, part_out), (core, part_keep)):
            for s in range(2):
                start = pl.multiple_of((2 * s + c) * width, width)
                target[k, s] = dot(hidden, wd[:, pl.ds(start, width)]).astype(bf16)
            if target is part_out:
                sum_core(k).start()

    def E(k):
        sum_core(k).wait_recv()
        y_out[k] = (
            part_keep[k, other_side].astype(f32) + part_in[k, other_side].astype(f32)
        ).astype(bf16)
        sum_side(k).start()
        y_own[k] = part_keep[k, side].astype(f32) + part_in[k, side].astype(f32)

    def F(k, own):
        sum_side(k).wait_recv()
        final[k] = (y_own[k] + y_in[k].astype(f32)).astype(bf16)
        if own:
            total[...] = dot(mix[me], final[0])
        else:
            give_back(k).start()

    def G(k):
        give_back(k).wait_recv()
        total[...] += dot(mix[flip(me, k, n_ep)], back[k])

    def rope_tables():
        lanes = lax.rem(iota((GRID_W, pair), 1), HEAD_DIM // 2)
        quarter = HEAD_DIM // 4
        inverse = jnp.exp(lax.rem(lanes, quarter).astype(f32) * (-LOG_BASE / quarter))
        by_row = lanes < quarter
        grid_rows = tokens // GRID_W
        first = me * grid_rows
        col_angle = iota((GRID_W, pair), 0).astype(f32) * inverse
        row_angle = (iota((grid_rows, pair), 0) + first).astype(f32) * inverse[0:grid_rows]
        for table, fn in ((ctab, jnp.cos), (stab, jnp.sin)):
            cols, rows = fn(col_angle), fn(row_angle)
            for r in range(grid_rows):
                table[r * GRID_W : (r + 1) * GRID_W, :] = jnp.where(
                    by_row, rows[r : r + 1, :], cols
                )

    def qkv():
        step = min(256, tokens)
        lanes = iota((1, pair), 1)
        low = lax.rem(lanes, HEAD_DIM) < HEAD_DIM // 2
        ones = one_zero(
            lax.rem(iota((2 * pair, pair), 0), pair) // HEAD_DIM
            == iota((2 * pair, pair), 1) // HEAD_DIM
        )
        gain_q = jnp.concatenate([q_gain[...]] * (pair // HEAD_DIM), axis=1)
        gain_k = jnp.concatenate([k_gain[...]] * (pair // HEAD_DIM), axis=1)

        def turned(x, gain, rows):
            square = x * x
            high = square.astype(bf16)
            rest = (square - high.astype(f32)).astype(bf16)
            mean = dot(jnp.concatenate([high, rest], axis=1), ones) * (1.0 / HEAD_DIM)
            scaled = x * lax.rsqrt(mean + EPSILON) * gain
            swapped = jnp.where(
                low,
                -pltpu.roll(scaled, pair - HEAD_DIM // 2, 1),
                pltpu.roll(scaled, HEAD_DIM // 2, 1),
            )
            return scaled * ctab[rows, :] + swapped * stab[rows, :]

        def body(i, carry):
            rows = pl.ds(pl.multiple_of(i * step, step), step)
            x = dot(xa[rows, :], wqkv[...])
            for g in range(q_cols // pair):
                span = slice(g * pair, (g + 1) * pair)
                q_s[rows, span] = (
                    turned(x[:, span], gain_q, rows) * HEAD_DIM ** (-0.5)
                ).astype(bf16)
            for g in range(kw // pair):
                span = slice(g * pair, (g + 1) * pair)
                k_span = slice(q_cols + g * pair, q_cols + (g + 1) * pair)
                kv[rows, span] = turned(x[:, k_span], gain_k, rows).astype(bf16)
            kv[rows, kw : 2 * kw] = x[:, q_cols + kw :].astype(bf16)
            return carry

        lax.fori_loop(0, tokens // step, body, 0)

    def expand(src, start, rows):
        block = jnp.concatenate([src[:, 0:kw], src[:, kw : 2 * kw]], axis=0)
        source = iota((kw, kv_local * pair), 0)
        column = iota((kw, kv_local * pair), 1)
        spread = one_zero(source == column // pair * HEAD_DIM + lax.rem(column, HEAD_DIM))
        doubled = dot(block, spread).astype(bf16)
        for h in range(kv_local):
            span = slice(h * pair, (h + 1) * pair)
            kd[h, start : start + rows, :] = doubled[0:rows, span]
            ve[h, start : start + rows, 0:pair] = doubled[rows:, span]
            ve[h, start : start + rows, pair : 2 * pair] = jnp.ones((rows, pair), bf16)

    def blank(start):
        for h in range(kv_local):
            kd[h, start : start + WINDOW, :] = jnp.zeros((WINDOW, pair), bf16)
            ve[h, start : start + WINDOW, :] = jnp.zeros((WINDOW, 2 * pair), bf16)

    def halo_start():
        @pl.when(me < n_ep - 1)
        def _():
            halo_up().start()

        @pl.when(me > 0)
        def _():
            halo_down().start()

    def halo_finish():
        @pl.when(me > 0)
        def _():
            halo_up().wait_recv()
            expand(halo.at[0], 0, WINDOW)

        @pl.when(me == 0)
        def _():
            blank(0)

        @pl.when(me < n_ep - 1)
        def _():
            halo_down().wait_recv()
            expand(halo.at[1], WINDOW + tokens, WINDOW)

        @pl.when(me == n_ep - 1)
        def _():
            blank(WINDOW + tokens)

    def attend(first, count, stride):
        span = 3 * WINDOW
        lanes = iota((1, pair), 1)
        left = one_zero(lanes < HEAD_DIM)
        right = one_zero(lanes >= HEAD_DIM)
        query = lax.rem(iota((2 * WINDOW, span), 0), WINDOW)
        key = iota((2 * WINDOW, span), 1)
        seen = (key >= query) & (key <= query + 2 * WINDOW)

        def body(j, carry):
            start = pl.multiple_of((first + stride * j) * WINDOW, WINDOW)
            rows = pl.ds(start, WINDOW)
            keys = pl.ds(start, span)
            for h in range(kv_local):
                cols = slice(h * pair, (h + 1) * pair)
                heads = q_s[rows, cols]
                stacked = jnp.concatenate([heads * left, heads * right], axis=0)
                scores = dot_nt(stacked, kd[h, keys, :])
                weights = jnp.where(seen, jnp.exp(scores), 0.0).astype(bf16)
                mixed = dot(weights, ve[h, keys, :])
                sink_0 = jnp.exp(jnp.full((1, pair), sink[2 * h], f32))
                sink_1 = jnp.exp(jnp.full((1, pair), sink[2 * h + 1], f32))
                upper = mixed[0:WINDOW, 0:pair] / (mixed[0:WINDOW, pair:] + sink_0)
                lower = mixed[WINDOW:, 0:pair] / (mixed[WINDOW:, pair:] + sink_1)
                att[rows, cols] = jnp.where(lanes < HEAD_DIM, upper, lower).astype(bf16)
            return carry

        lax.fori_loop(0, count, body, 0)

    def project():
        tile = 2 * pair
        quarter = attn_ref.shape[1]

        def body(n, carry):
            cols = pl.ds(pl.multiple_of(n * tile, tile), tile)
            x = dot(att[...], wo[:, cols]).astype(bf16)
            for s in range(attn_ref.shape[0]):
                attn_ref[s, :, cols] = x[s * quarter : (s + 1) * quarter]
            return carry

        lax.fori_loop(0, wo.shape[1] // tile, body, 0)
        attn_core(0).start()
        attn_core(1).start()

    def attn_sum():
        attn_core(0).wait_recv()
        attn_core(1).wait_recv()

    def attn_cross(c):
        rows = slice(c * chunk_rows, (c + 1) * chunk_rows)
        attn_y_out[c] = (
            attn_ref[2 * other_side + core, rows].astype(f32)
            + attn_in[other_side, rows].astype(f32)
        ).astype(bf16)
        attn_side(c).start()

    def attn_final(c):
        rows = slice(c * chunk_rows, (c + 1) * chunk_rows)
        attn_side(c).wait_recv()
        attn_out_ref[rows] = (
            attn_ref[2 * side + core, rows].astype(f32)
            + attn_in[side, rows].astype(f32)
            + attn_y_in[c].astype(f32)
        ).astype(bf16)

    nb = tokens // WINDOW

    plan()
    loads[0].wait()
    for copy in loads[1:]:
        copy.start()
    rms_inplace(xe, e_gain, 32)
    pl.semaphore_wait(barrier, n_ep + 1)

    def load_ffn():
        for copy in loads[1:4]:
            copy.wait()

    def attention_front():
        for copy in loads[4:9]:
            copy.wait()
        rms_inplace(xa, a_gain, 32)
        rope_tables()
        qkv()

    if n_ep == 8:
        D(4, False)
        D(1, True)
        D(5, False)
        D(2, True)
        L0()
        load_ffn()
        C(0)
        attention_front()
        E(0)
        halo_start()
        D(6, False)
        D(3, True)
        D(7, False)
        expand(kv, WINDOW, tokens)
        attend(1, nb - 2, 1)
        A(1, True)
        A(4, False)
        C(1)
        build_mix()
        E(1)
        B(4)
        C(4)
        halo_finish()
        attend(0, 2, nb - 1)
        E(4)
        project()
        F(0, True)
        A(2, True)
        F(1, False)
        C(2)
        A(5, False)
        F(4, False)
        E(2)
        attn_sum()
        attn_cross(0)
        B(5)
        C(5)
        A(3, True)
        E(5)
        F(2, False)
        C(3)
        A(6, False)
        E(3)
        F(5, False)
        attn_cross(1)
        B(6)
        C(6)
        F(3, False)
        E(6)
        attn_cross(2)
        G(1)
        A(7, False)
        F(6, False)
        B(7)
        C(7)
        E(7)
        attn_cross(3)
        G(4)
        G(2)
        F(7, False)
        G(5)
        G(3)
        for c in range(ATTN_CHUNKS):
            attn_final(c)
        G(6)
        G(7)
    else:
        def each(low, high, fn):
            def body(k, carry):
                fn(k)
                return carry

            lax.fori_loop(low, high, body, 0)

        each(half, n_ep, lambda k: D(k, False))
        each(1, half, lambda k: D(k, True))
        L0()
        load_ffn()
        attention_front()
        halo_start()
        expand(kv, WINDOW, tokens)
        attend(1, nb - 2, 1)
        each(1, half, lambda k: A(k, True))
        each(half, n_ep, lambda k: A(k, False))
        halo_finish()
        attend(0, 2, nb - 1)
        project()
        build_mix()
        each(half, n_ep, B)
        each(0, n_ep, C)
        each(0, n_ep, E)
        attn_sum()
        F(0, True)
        each(1, n_ep, lambda k: F(k, False))
        for c in range(ATTN_CHUNKS):
            attn_cross(c)
        each(1, n_ep, G)
        for c in range(ATTN_CHUNKS):
            attn_final(c)

    out_ref[...] = total[...].astype(bf16)

    def drain(k, carry):
        @pl.when(k > 0)
        def _():
            dispatch(k).wait_send()
            give_back(k).wait_send()

        to_partner(k).wait_send()

        @pl.when(k >= half)
        def _():
            to_across(k).wait_send()

        @pl.when((k > 0) & (k < half))
        def _():
            dispatch_other(k).wait_send()

        relay(k).wait_send()
        sum_core(k).wait_send()
        sum_side(k).wait_send()
        return carry

    lax.fori_loop(0, n_ep, drain, 0)
    attn_core(0).wait_send()
    attn_core(1).wait_send()
    for c in range(ATTN_CHUNKS):
        attn_side(c).wait_send()

    @pl.when(me < n_ep - 1)
    def _():
        halo_up().wait_send()

    @pl.when(me > 0)
    def _():
        halo_down().wait_send()


def per_device(
    x_attend, attend_gain, w_query, w_key, w_value, query_gain, key_gain, sink_logit, w_output,
    x_experts, expert_gain, routes, group_prob, expert_prob, w_gate, w_up, w_down,
):
    tokens, model_width = x_attend.shape
    q_cols, kv_cols = w_query.shape[1], w_key.shape[1]
    kv_local = kv_cols // HEAD_DIM
    tp_count, n_ep = lax.axis_size("tp"), lax.axis_size("ep")
    moe_rows, top_count = routes.shape
    capacity = max(2, (3 * moe_rows * top_count + 2 * n_ep - 1) // (2 * n_ep))
    col_width = model_width // tp_count
    hidden_cols = w_gate.shape[2]
    slice_rows = tokens // tp_count
    ext = tokens + 2 * WINDOW
    pair = 2 * HEAD_DIM
    chunk = slice_rows // ATTN_CHUNKS
    vmem = pl.BlockSpec(memory_space=pltpu.VMEM)
    smem = pl.BlockSpec(memory_space=pltpu.SMEM)
    hbm = pl.BlockSpec(memory_space=pl.ANY)
    dma = pltpu.SemaphoreType.DMA

    def buf(*shape, dtype=bf16):
        return pltpu.VMEM(shape, dtype)

    expert_out, attend_out = pl.pallas_call(
        functools.partial(fused_kernel, n_ep),
        out_shape=(
            jax.ShapeDtypeStruct((moe_rows, col_width), bf16),
            jax.ShapeDtypeStruct((slice_rows, model_width), bf16),
        ),
        in_specs=[
            hbm, vmem, hbm, hbm, hbm, vmem, vmem, smem, hbm,
            hbm, vmem, vmem, vmem, vmem, hbm, hbm, hbm,
        ],
        out_specs=(vmem, vmem),
        scratch_shapes=[
            buf(tokens, model_width),
            buf(model_width, q_cols + 2 * kv_cols),
            buf(q_cols, model_width),
            buf(moe_rows, model_width),
            buf(model_width, 2 * hidden_cols),
            buf(hidden_cols, model_width),
            buf(tokens, pair, dtype=f32),
            buf(tokens, pair, dtype=f32),
            buf(tokens, q_cols),
            buf(tokens, 2 * kv_cols),
            buf(2, WINDOW, 2 * kv_cols),
            buf(kv_local, ext, pair),
            buf(kv_local, ext, 2 * pair),
            buf(tokens, q_cols),
            buf(tp_count, slice_rows, model_width),
            buf(2, slice_rows, model_width),
            buf(ATTN_CHUNKS, chunk, model_width),
            buf(ATTN_CHUNKS, chunk, model_width),
            buf(n_ep, moe_rows, dtype=f32),
            buf(moe_rows, n_ep, dtype=f32),
            buf(moe_rows, n_ep, dtype=f32),
            buf(n_ep, moe_rows, capacity),
            buf(n_ep, capacity, col_width),
            buf(n_ep // 2, capacity, col_width),
            buf(tp_count, n_ep, capacity, col_width),
            buf(n_ep, 2, capacity, col_width),
            buf(n_ep, 2, capacity, col_width),
            buf(n_ep, 2, capacity, col_width),
            buf(n_ep, capacity, col_width),
            buf(n_ep, capacity, col_width, dtype=f32),
            buf(n_ep, capacity, col_width),
            buf(n_ep, capacity, col_width),
            buf(n_ep, capacity, col_width),
            buf(moe_rows, col_width, dtype=f32),
            dma((9,)),
        ]
        + [dma((n_ep,))] * 16
        + [dma((2,))] * 2
        + [dma((ATTN_CHUNKS,))] * 2
        + [dma((2,))] * 2,
        compiler_params=pltpu.CompilerParams(
            collective_id=0, has_side_effects=True, vmem_limit_bytes=60 * 1024 * 1024
        ),
    )(
        x_attend, attend_gain[None], w_query, w_key, w_value, query_gain[None], key_gain[None],
        sink_logit, w_output, x_experts, expert_gain[None], routes.T, group_prob[None],
        expert_prob.T, w_gate[0], w_up[0], w_down[0],
    )
    return (attend_out, expert_out)


def solution(mesh):
    placed = (
        P("ep", None),
        P(),
        P(None, "tp"),
        P(None, "tp"),
        P(None, "tp"),
        P(),
        P(),
        P("tp"),
        P("tp", None),
        P("ep", None),
        P(),
        P("ep", None),
        P("ep"),
        P("ep", None),
        P("ep", None, "tp"),
        P("ep", None, "tp"),
        P("ep", "tp", None),
    )
    return jax.shard_map(
        per_device,
        mesh=mesh,
        in_specs=placed,
        out_specs=(P(("ep", "tp"), None), P("ep", "tp")),
        check_vma=False,
    )
```

time: 117 us -> 89.4 us (0.76)
  matrix products: 14.9 us -> 0 us
  other arithmetic: 14.2 us -> 0 us
  Pallas kernels: 74.5 us -> 83.6 us
  starting transfers between devices: 6.95 us -> 0 us
    dot_general x7 -> x0, matrix products: 14.9 us -> none  [the longest x1 4.7 us: per_device(): jnp.einsum('hgqk,khd->qhgd', probs, span_values, preferred_element_type=j...]
    pallas_call x1, Pallas kernels: 74.5 us -> 83.6 us  [per_device(): pl.pallas_call(functools.partial(fused_kernel, n_ep), out_shape=(jax.Shap...]
    ppermute x2 -> x0, starting transfers between devices: 6.95 us -> none  [the longest x1 5.49 us: extended(): before = lax.ppermute(last, axis, up)]
    convert_element_type x4 -> x0, other arithmetic: 5.08 us -> none  [the longest x1 2.34 us: per_device(): mix = jnp.where(rank.T[:, :, None] == slots[None, None, :], share.T[:, :,...]
    reduce_sum x5 -> x0, other arithmetic: 3.94 us -> none  [the longest x2 2.54 us: rms_scale(): jnp.mean(values_f * values_f, axis=-1, keepdims=True) + epsilon]
    unnamed x28 -> x2, local copies, waits for them, and re-layouts: 4.91 us -> 3.65 us
    broadcast_in_dim x0 -> x1, local copies, waits for them, and re-layouts: none -> 1.25 us  [per_device(): group_prob[None]]
  transfers between devices with their start and end apart: 2 -> 0, of which waited for: 0 -> 0; matrix products, arithmetic and copies ran while one was open for 9% -> 0% of each run, Pallas kernels for 0% -> 0%
where the time goes in v1:
time: 89.4 us; the launch traced here: 89.1 us
  Pallas kernels  83.6 us (94%)
  local copies, waits for them, and re-layouts  4.89 us (5%)
    pallas_call x1, Pallas kernels, per_device(): pl.pallas_call(functools.partial(fused_kernel, n_ep), out_shape=(jax.Shap...  83.6 us
    unnamed x2, local copies, waits for them, and re-layouts  3.65 us

profile of v1, /device:TPU:0, one launch (start us, length us, event | category | flops | bytes accessed | tf_op | source)
XLA Modules:
  0.0 89.1 jit_solution(13574550080572959436)
XLA Ops:
  0.6 1.2 %broadcast_in_dim.19.group_p = f32[1,384]{1,0:T(1,128)} reshape(f32[384]{0:T(512)} %param.29) | data formatting | bytes 3072 | tf_op jit(solution)/shard_map/broadcast_in_dim | solution.py:682
  1.9 83.6 %shard_map.176 = (bf16[384,512]{1,0:T(8,128)(2,1)}, bf16[128,2048]{1,0:T(8,128)(2,1)}) custom-call(bf16[512,2048]{1,0:T(8,128)(2,1)} %xa_hbm.1, f32[1,2048]{1,0:T(1,128)} %bitcast.12, bf16[2048,256]{1,0:T(8,128)(2,1)} %wq_hbm.1, bf16[2048,128]{1,0:T(8,128)(2,1)} %wk_hbm.1, bf16[2048,128]{1,0:T(8,128)(2,1)} %wv_hbm.1, f32[1,64]{1,0:T(1,128)} %bitcast.16, ...), custom_call_target="tpu_custom_call" | custom-call | tf_op jit(solution)/shard_map/pallas_call | solution.py:625
  85.5 1.9 %copy.21 = bf16[128,2048]{1,0:T(8,128)(2,1)} copy(bf16[128,2048]{1,0:T(8,128)(2,1)} %get-tuple-element.8) | data formatting | bytes 1048576
  87.3 1.8 %copy.22 = bf16[384,512]{1,0:T(8,128)(2,1)} copy(bf16[384,512]{1,0:T(8,128)(2,1)} %get-tuple-element.9) | data formatting | bytes 786432

commit v2 on v1

--- a/solution.py
+++ b/solution.py
@@ -13,7 +13,8 @@
 MESH = pl.DeviceIdType.MESH
 EPSILON = 1e-06
 LOG_BASE = 9.210340371976184
-ATTN_CHUNKS = 4
+ATTN_CHUNKS = 8
+XE_PIECES = 3
 bf16, f32, i32 = jnp.bfloat16, jnp.float32, jnp.int32
 
 
@@ -41,29 +42,31 @@
     return jnp.where(mask, 1.0, 0.0).astype(bf16)
 
 
-def rms_inplace(ref, gain_ref, chunk):
+def rms_inplace(ref, first, count, gain_ref):
+    chunk = 32
+
     def body(i, carry):
-        rows = pl.ds(pl.multiple_of(i * chunk, chunk), chunk)
+        rows = pl.ds(pl.multiple_of(first + i * chunk, chunk), chunk)
         v = ref[rows, :].astype(f32)
         scale = lax.rsqrt(jnp.mean(v * v, axis=-1, keepdims=True) + EPSILON)
         ref[rows, :] = (v * scale * gain_ref[...]).astype(bf16)
         return carry
 
-    lax.fori_loop(0, ref.shape[0] // chunk, body, 0)
+    lax.fori_loop(0, count // chunk, body, 0)
 
 
 def fused_kernel(
     n_ep,
     xa_hbm, a_gain, wq_hbm, wk_hbm, wv_hbm, q_gain, k_gain, sink, wo_hbm,
-    xe_hbm, e_gain, routes_t, group_p, expert_p, wg_hbm, wu_hbm, wd_hbm,
+    xe_hbm, e_gain, routes_t, group_hbm, expert_p, wg_hbm, wu_hbm, wd_hbm,
     out_ref, attn_out_ref,
     xa, wqkv, wo, xe, wgu, wd,
     ctab, stab, q_s, kv, halo, kd, ve, att,
     attn_ref, attn_in, attn_y_out, attn_y_in,
-    rank_s, rank_tn, share_tn, mix,
+    group_p, rank_s, rank_tn, share_tn, mix,
     send_own, send_other, rows_buf, part_out, part_keep, part_in,
     y_out, y_own, y_in, final, back, total,
-    l_sem,
+    l_sem, x_sem,
     d_send, d_recv, e_send, e_recv, p_send, p_recv, y_send, y_recv,
     r_send, r_recv, c_send, c_recv, s_send, s_recv, f_send, f_recv,
     a_send, a_recv, b_send, b_recv, h_send, h_recv,
@@ -88,17 +91,28 @@
 
     kw = wk_hbm.shape[1]
     loads = [
-        local(0, xe_hbm, xe),
-        local(1, wg_hbm, wgu.at[:, 0:hidden_cols]),
-        local(2, wu_hbm, wgu.at[:, hidden_cols : 2 * hidden_cols]),
-        local(3, wd_hbm, wd),
-        local(4, xa_hbm, xa),
-        local(5, wq_hbm, wqkv.at[:, 0:q_cols]),
-        local(6, wk_hbm, wqkv.at[:, q_cols : q_cols + kw]),
-        local(7, wv_hbm, wqkv.at[:, q_cols + kw : q_cols + 2 * kw]),
-        local(8, wo_hbm, wo),
+        local(0, wg_hbm, wgu.at[:, 0:hidden_cols]),
+        local(1, wu_hbm, wgu.at[:, hidden_cols : 2 * hidden_cols]),
+        local(2, wd_hbm, wd),
+        local(3, xa_hbm, xa),
+        local(4, wq_hbm, wqkv.at[:, 0:q_cols]),
+        local(5, wk_hbm, wqkv.at[:, q_cols : q_cols + kw]),
+        local(6, wv_hbm, wqkv.at[:, q_cols + kw : q_cols + 2 * kw]),
+        local(7, wo_hbm, wo),
+        local(8, group_hbm, group_p.at[0]),
     ]
-    loads[0].start()
+    loads[8].start()
+    first_rows = moe_tokens // XE_PIECES
+    pieces = [
+        pltpu.make_async_copy(
+            xe_hbm.at[i * first_rows : (i + 1) * first_rows],
+            xe.at[i * first_rows : (i + 1) * first_rows],
+            x_sem.at[i],
+        )
+        for i in range(XE_PIECES)
+    ]
+    for copy in pieces:
+        copy.start()
 
     barrier = pltpu.get_barrier_semaphore()
 
@@ -226,13 +240,13 @@
 
     def A(k, near):
         dispatch(k).wait_recv()
-        if near:
-            to_partner(k).start()
-            dispatch_other(k).wait_recv()
-            relay(k).start()
-        else:
+        if not near:
             to_across(k).start()
-            to_partner(k).start()
+        to_partner(k).start()
+
+    def Z(k):
+        dispatch_other(k).wait_recv()
+        relay(k).start()
 
     def B(k):
         to_across(k).wait_recv()
@@ -441,91 +455,111 @@
 
     nb = tokens // WINDOW
 
+    loads[8].wait()
     plan()
-    loads[0].wait()
-    for copy in loads[1:]:
-        copy.start()
-    rms_inplace(xe, e_gain, 32)
+    for i, copy in enumerate(pieces):
+        copy.wait()
+        if i == XE_PIECES - 1:
+            for load in loads[0:8]:
+                load.start()
+        rms_inplace(xe, i * first_rows, first_rows, e_gain)
     pl.semaphore_wait(barrier, n_ep + 1)
 
     def load_ffn():
-        for copy in loads[1:4]:
+        for copy in loads[0:3]:
             copy.wait()
 
-    def attention_front():
-        for copy in loads[4:9]:
+    def front_norm():
+        loads[3].wait()
+        rms_inplace(xa, 0, tokens, a_gain)
+
+    def front_qkv():
+        for copy in loads[4:8]:
             copy.wait()
-        rms_inplace(xa, a_gain, 32)
         rope_tables()
         qkv()
 
     if n_ep == 8:
+        D(1, True)
         D(4, False)
-        D(1, True)
-        D(5, False)
         D(2, True)
         L0()
+        front_norm()
+        front_qkv()
+        halo_start()
+        expand(kv, WINDOW, tokens)
+        D(6, False)
         load_ffn()
         C(0)
-        attention_front()
+        D(5, False)
+        A(1, True)
+        Z(1)
+        attend(1, nb - 2, 1)
         E(0)
-        halo_start()
-        D(6, False)
+        C(1)
+        A(4, False)
+        build_mix()
+        A(2, True)
+        Z(2)
+        C(2)
+        D(7, False)
+        E(1)
         D(3, True)
-        D(7, False)
-        expand(kv, WINDOW, tokens)
-        attend(1, nb - 2, 1)
-        A(1, True)
-        A(4, False)
-        C(1)
-        build_mix()
-        E(1)
-        B(4)
-        C(4)
         halo_finish()
         attend(0, 2, nb - 1)
+        E(2)
+        B(4)
+        project()
+        A(6, False)
+        attn_sum()
+        C(4)
         E(4)
-        project()
         F(0, True)
-        A(2, True)
+        B(6)
+        A(5, False)
+        C(6)
+        attn_cross(0)
+        E(6)
+        F(4, False)
+        A(3, True)
+        Z(3)
+        F(2, False)
+        A(7, False)
+        attn_cross(4)
         F(1, False)
-        C(2)
-        A(5, False)
-        F(4, False)
-        E(2)
-        attn_sum()
-        attn_cross(0)
         B(5)
         C(5)
-        A(3, True)
+        F(6, False)
+        C(3)
+        attn_final(0)
         E(5)
-        F(2, False)
-        C(3)
-        A(6, False)
-        E(3)
+        attn_cross(7)
+        B(7)
+        G(1)
+        C(7)
+        G(4)
+        attn_cross(2)
+        attn_final(4)
+        E(7)
         F(5, False)
-        attn_cross(1)
-        B(6)
-        C(6)
-        F(3, False)
-        E(6)
-        attn_cross(2)
-        G(1)
-        A(7, False)
-        F(6, False)
-        B(7)
-        C(7)
-        E(7)
-        attn_cross(3)
-        G(4)
         G(2)
         F(7, False)
+        E(3)
+        attn_cross(3)
+        attn_cross(6)
+        attn_cross(1)
+        F(3, False)
+        G(6)
         G(5)
+        attn_final(3)
+        attn_final(2)
+        attn_cross(5)
+        G(7)
+        attn_final(5)
+        attn_final(6)
+        attn_final(7)
+        attn_final(1)
         G(3)
-        for c in range(ATTN_CHUNKS):
-            attn_final(c)
-        G(6)
-        G(7)
     else:
         def each(low, high, fn):
             def body(k, carry):
@@ -538,11 +572,13 @@
         each(1, half, lambda k: D(k, True))
         L0()
         load_ffn()
-        attention_front()
+        front_norm()
+        front_qkv()
         halo_start()
         expand(kv, WINDOW, tokens)
         attend(1, nb - 2, 1)
         each(1, half, lambda k: A(k, True))
+        each(1, half, Z)
         each(half, n_ep, lambda k: A(k, False))
         halo_finish()
         attend(0, 2, nb - 1)
@@ -624,13 +660,10 @@
 
     expert_out, attend_out = pl.pallas_call(
         functools.partial(fused_kernel, n_ep),
-        out_shape=(
-            jax.ShapeDtypeStruct((moe_rows, col_width), bf16),
-            jax.ShapeDtypeStruct((slice_rows, model_width), bf16),
-        ),
+        out_shape=(buf(moe_rows, col_width), buf(slice_rows, model_width)),
         in_specs=[
             hbm, vmem, hbm, hbm, hbm, vmem, vmem, smem, hbm,
-            hbm, vmem, vmem, vmem, vmem, hbm, hbm, hbm,
+            hbm, vmem, vmem, hbm, vmem, hbm, hbm, hbm,
         ],
         out_specs=(vmem, vmem),
         scratch_shapes=[
@@ -652,6 +685,7 @@
             buf(2, slice_rows, model_width),
             buf(ATTN_CHUNKS, chunk, model_width),
             buf(ATTN_CHUNKS, chunk, model_width),
+            buf(1, moe_rows, dtype=f32),
             buf(n_ep, moe_rows, dtype=f32),
             buf(moe_rows, n_ep, dtype=f32),
             buf(moe_rows, n_ep, dtype=f32),
@@ -669,6 +703,7 @@
             buf(n_ep, capacity, col_width),
             buf(moe_rows, col_width, dtype=f32),
             dma((9,)),
+            dma((XE_PIECES,)),
         ]
         + [dma((n_ep,))] * 16
         + [dma((2,))] * 2
@@ -679,7 +714,7 @@
         ),
     )(
         x_attend, attend_gain[None], w_query, w_key, w_value, query_gain[None], key_gain[None],
-        sink_logit, w_output, x_experts, expert_gain[None], routes.T, group_prob[None],
+        sink_logit, w_output, x_experts, expert_gain[None], routes.T, group_prob,
         expert_prob.T, w_gate[0], w_up[0], w_down[0],
     )
     return (attend_out, expert_out)

time: 89.4 us -> 73.5 us (0.82)
  Pallas kernels: 83.6 us -> 71.1 us
  local copies, waits for them, and re-layouts: 4.89 us -> 1.54 us
    pallas_call x1, Pallas kernels: 83.6 us -> 71.1 us  [per_device(): pl.pallas_call(functools.partial(fused_kernel, n_ep), out_shape=(buf(moe_...]
    unnamed x2, local copies, waits for them, and re-layouts: 3.65 us -> 1.54 us
    broadcast_in_dim x1 -> x0, local copies, waits for them, and re-layouts: 1.25 us -> none  [per_device(): group_prob[None]]
where the time goes in v2:
time: 73.5 us; the launch traced here: 73.3 us
  Pallas kernels  71.1 us (97%)
  local copies, waits for them, and re-layouts  1.54 us (2%)
    pallas_call x1, Pallas kernels, per_device(): pl.pallas_call(functools.partial(fused_kernel, n_ep), out_shape=(buf(moe_...  71.1 us
    unnamed x2, local copies, waits for them, and re-layouts  1.54 us

profile of v2, /device:TPU:0, one launch (start us, length us, event | category | flops | bytes accessed | tf_op | source)
XLA Modules:
  0.0 73.3 jit_solution(5416770952454852150)
XLA Ops:
  0.6 71.1 %shard_map.176 = (bf16[384,512]{1,0:T(8,128)(2,1)S(1)}, bf16[128,2048]{1,0:T(8,128)(2,1)S(1)}) custom-call(bf16[512,2048]{1,0:T(8,128)(2,1)} %xa_hbm.1, f32[1,2048]{1,0:T(1,128)} %bitcast.12, bf16[2048,256]{1,0:T(8,128)(2,1)} %wq_hbm.1, bf16[2048,128]{1,0:T(8,128)(2,1)} %wk_hbm.1, bf16[2048,128]{1,0:T(8,128)(2,1)} %wv_hbm.1, f32[1,64]{1,0:T(1,128)} %bitcast.16, ...), custom_call_target="tpu_custom_call" | custom-call | tf_op jit(solution)/shard_map/pallas_call | solution.py:661
  71.8 0.8 %copy.21 = bf16[128,2048]{1,0:T(8,128)(2,1)} copy(bf16[128,2048]{1,0:T(8,128)(2,1)S(1)} %get-tuple-element.6) | data formatting | bytes 1048576
  72.6 0.7 %copy.22 = bf16[384,512]{1,0:T(8,128)(2,1)} copy(bf16[384,512]{1,0:T(8,128)(2,1)S(1)} %get-tuple-element.7) | data formatting | bytes 786432

commit v3 on v2

--- a/solution.py
+++ b/solution.py
@@ -43,30 +43,39 @@
 
 
 def rms_inplace(ref, first, count, gain_ref):
-    chunk = 32
+    chunk, lanes = 64, 128
+    features = ref.shape[1]
+    steps = 2 if count % (2 * chunk) == 0 else 1
 
     def body(i, carry):
-        rows = pl.ds(pl.multiple_of(first + i * chunk, chunk), chunk)
-        v = ref[rows, :].astype(f32)
-        scale = lax.rsqrt(jnp.mean(v * v, axis=-1, keepdims=True) + EPSILON)
-        ref[rows, :] = (v * scale * gain_ref[...]).astype(bf16)
+        for j in range(steps):
+            start = first + (i * steps + j) * chunk
+            rows = pl.ds(pl.multiple_of(start, chunk), chunk)
+            v = ref[rows, :].astype(f32)
+            square = v * v
+            part = square[:, 0:lanes]
+            for c in range(lanes, features, lanes):
+                part = part + square[:, c : c + lanes]
+            mean = jnp.sum(part, axis=-1, keepdims=True) * (1.0 / features)
+            ref[rows, :] = (v * lax.rsqrt(mean + EPSILON) * gain_ref[...]).astype(bf16)
         return carry
 
-    lax.fori_loop(0, count // chunk, body, 0)
+    lax.fori_loop(0, count // (chunk * steps), body, 0)
 
 
 def fused_kernel(
     n_ep,
-    xa_hbm, a_gain, wq_hbm, wk_hbm, wv_hbm, q_gain, k_gain, sink, wo_hbm,
-    xe_hbm, e_gain, routes_t, group_hbm, expert_p, wg_hbm, wu_hbm, wd_hbm,
+    xa_hbm, a_gain_hbm, wq_hbm, wk_hbm, wv_hbm, q_gain_hbm, k_gain_hbm, sink_hbm, wo_hbm,
+    xe_hbm, e_gain_hbm, routes_hbm, group_hbm, expert_hbm, wg_hbm, wu_hbm, wd_hbm,
     out_ref, attn_out_ref,
     xa, wqkv, wo, xe, wgu, wd,
     ctab, stab, q_s, kv, halo, kd, ve, att,
     attn_ref, attn_in, attn_y_out, attn_y_in,
+    a_gain, q_gain, k_gain, sink, e_gain, routes_t, expert_p,
     group_p, rank_s, rank_tn, share_tn, mix,
     send_own, send_other, rows_buf, part_out, part_keep, part_in,
     y_out, y_own, y_in, final, back, total,
-    l_sem, x_sem,
+    l_sem, x_sem, s_sem,
     d_send, d_recv, e_send, e_recv, p_send, p_recv, y_send, y_recv,
     r_send, r_recv, c_send, c_recv, s_send, s_recv, f_send, f_recv,
     a_send, a_recv, b_send, b_recv, h_send, h_recv,
@@ -99,9 +108,24 @@
         local(5, wk_hbm, wqkv.at[:, q_cols : q_cols + kw]),
         local(6, wv_hbm, wqkv.at[:, q_cols + kw : q_cols + 2 * kw]),
         local(7, wo_hbm, wo),
-        local(8, group_hbm, group_p.at[0]),
     ]
-    loads[8].start()
+    small = [
+        pltpu.make_async_copy(src, dst, s_sem.at[i])
+        for i, (src, dst) in enumerate(
+            [
+                (routes_hbm, routes_t),
+                (expert_hbm, expert_p),
+                (group_hbm, group_p.at[0]),
+                (e_gain_hbm, e_gain.at[0]),
+                (a_gain_hbm, a_gain.at[0]),
+                (q_gain_hbm, q_gain.at[0]),
+                (k_gain_hbm, k_gain.at[0]),
+                (sink_hbm, sink),
+            ]
+        )
+    ]
+    for copy in small:
+        copy.start()
     first_rows = moe_tokens // XE_PIECES
     pieces = [
         pltpu.make_async_copy(
@@ -455,7 +479,8 @@
 
     nb = tokens // WINDOW
 
-    loads[8].wait()
+    for copy in small[0:4]:
+        copy.wait()
     plan()
     for i, copy in enumerate(pieces):
         copy.wait()
@@ -470,6 +495,8 @@
             copy.wait()
 
     def front_norm():
+        for copy in small[4:8]:
+            copy.wait()
         loads[3].wait()
         rms_inplace(xa, 0, tokens, a_gain)
 
@@ -480,86 +507,86 @@
         qkv()
 
     if n_ep == 8:
+        D(6, False)
+        L0()
         D(1, True)
         D(4, False)
+        front_norm()
         D(2, True)
-        L0()
-        front_norm()
-        front_qkv()
-        halo_start()
-        expand(kv, WINDOW, tokens)
-        D(6, False)
+        D(7, False)
         load_ffn()
         C(0)
+        front_qkv()
+        A(6, False)
+        build_mix()
+        E(0)
+        halo_start()
+        B(6)
+        A(4, False)
+        Z(1)
+        Z(2)
+        A(2, True)
+        C(6)
+        F(0, True)
+        E(6)
+        B(4)
         D(5, False)
+        D(3, True)
+        C(2)
+        A(7, False)
         A(1, True)
-        Z(1)
+        C(4)
+        E(2)
+        halo_finish()
+        expand(kv, WINDOW, tokens)
+        F(6, False)
+        E(4)
+        attend(0, 2, nb - 1)
         attend(1, nb - 2, 1)
-        E(0)
         C(1)
-        A(4, False)
-        build_mix()
-        A(2, True)
-        Z(2)
-        C(2)
-        D(7, False)
+        B(7)
+        project()
+        A(5, False)
+        A(3, True)
+        C(7)
         E(1)
-        D(3, True)
-        halo_finish()
-        attend(0, 2, nb - 1)
-        E(2)
-        B(4)
-        project()
-        A(6, False)
+        E(7)
+        F(4, False)
+        B(5)
+        G(6)
         attn_sum()
-        C(4)
-        E(4)
-        F(0, True)
-        B(6)
-        A(5, False)
-        C(6)
-        attn_cross(0)
-        E(6)
-        F(4, False)
-        A(3, True)
+        F(2, False)
         Z(3)
-        F(2, False)
-        A(7, False)
-        attn_cross(4)
+        C(5)
+        attn_cross(1)
+        C(3)
         F(1, False)
-        B(5)
-        C(5)
-        F(6, False)
-        C(3)
-        attn_final(0)
+        attn_cross(6)
         E(5)
-        attn_cross(7)
-        B(7)
-        G(1)
-        C(7)
-        G(4)
-        attn_cross(2)
-        attn_final(4)
-        E(7)
-        F(5, False)
-        G(2)
         F(7, False)
         E(3)
+        attn_cross(0)
+        G(2)
+        attn_final(1)
+        attn_cross(2)
+        F(5, False)
+        attn_cross(4)
+        F(3, False)
         attn_cross(3)
-        attn_cross(6)
-        attn_cross(1)
-        F(3, False)
-        G(6)
+        attn_cross(5)
+        attn_final(0)
+        G(4)
+        G(1)
+        attn_cross(7)
+        attn_final(5)
+        attn_final(6)
+        attn_final(4)
+        G(7)
+        attn_final(2)
         G(5)
         attn_final(3)
-        attn_final(2)
-        attn_cross(5)
-        G(7)
-        attn_final(5)
-        attn_final(6)
+        G(3)
         attn_final(7)
-        attn_final(1)
-        G(3)
     else:
         def each(low, high, fn):
             def body(k, carry):
@@ -651,7 +678,6 @@
     pair = 2 * HEAD_DIM
     chunk = slice_rows // ATTN_CHUNKS
     vmem = pl.BlockSpec(memory_space=pltpu.VMEM)
-    smem = pl.BlockSpec(memory_space=pltpu.SMEM)
     hbm = pl.BlockSpec(memory_space=pl.ANY)
     dma = pltpu.SemaphoreType.DMA
 
@@ -661,10 +687,7 @@
     expert_out, attend_out = pl.pallas_call(
         functools.partial(fused_kernel, n_ep),
         out_shape=(buf(moe_rows, col_width), buf(slice_rows, model_width)),
-        in_specs=[
-            hbm, vmem, hbm, hbm, hbm, vmem, vmem, smem, hbm,
-            hbm, vmem, vmem, hbm, vmem, hbm, hbm, hbm,
-        ],
+        in_specs=[hbm] * 17,
         out_specs=(vmem, vmem),
         scratch_shapes=[
             buf(tokens, model_width),
@@ -685,6 +708,13 @@
             buf(2, slice_rows, model_width),
             buf(ATTN_CHUNKS, chunk, model_width),
             buf(ATTN_CHUNKS, chunk, model_width),
+            buf(1, model_width, dtype=f32),
+            buf(1, HEAD_DIM, dtype=f32),
+            buf(1, HEAD_DIM, dtype=f32),
+            pltpu.SMEM(sink_logit.shape, f32),
+            buf(1, model_width, dtype=f32),
+            buf(top_count, moe_rows, dtype=i32),
+            buf(top_count, moe_rows, dtype=f32),
             buf(1, moe_rows, dtype=f32),
             buf(n_ep, moe_rows, dtype=f32),
             buf(moe_rows, n_ep, dtype=f32),
@@ -702,8 +732,9 @@
             buf(n_ep, capacity, col_width),
             buf(n_ep, capacity, col_width),
             buf(moe_rows, col_width, dtype=f32),
-            dma((9,)),
+            dma((8,)),
             dma((XE_PIECES,)),
+            dma((8,)),
         ]
         + [dma((n_ep,))] * 16
         + [dma((2,))] * 2
@@ -713,8 +744,8 @@
             collective_id=0, has_side_effects=True, vmem_limit_bytes=60 * 1024 * 1024
         ),
     )(
-        x_attend, attend_gain[None], w_query, w_key, w_value, query_gain[None], key_gain[None],
-        sink_logit, w_output, x_experts, expert_gain[None], routes.T, group_prob,
+        x_attend, attend_gain, w_query, w_key, w_value, query_gain, key_gain,
+        sink_logit, w_output, x_experts, expert_gain, routes.T, group_prob,
         expert_prob.T, w_gate[0], w_up[0], w_down[0],
     )
     return (attend_out, expert_out)

time: 73.5 us -> 71.6 us (0.974)
  Pallas kernels: 71.1 us -> 69.2 us
    pallas_call x1, Pallas kernels: 71.1 us -> 69.2 us  [per_device(): pl.pallas_call(functools.partial(fused_kernel, n_ep), out_shape=(buf(moe_...]
where the time goes in v3:
time: 71.6 us; the launch traced here: 71.4 us
  Pallas kernels  69.2 us (97%)
  local copies, waits for them, and re-layouts  1.54 us (2%)
    pallas_call x1, Pallas kernels, per_device(): pl.pallas_call(functools.partial(fused_kernel, n_ep), out_shape=(buf(moe_...  69.2 us
    unnamed x2, local copies, waits for them, and re-layouts  1.54 us

profile of v3, /device:TPU:0, one launch (start us, length us, event | category | flops | bytes accessed | tf_op | source)
XLA Modules:
  0.0 71.4 jit_solution(12226099152676154795)
XLA Ops:
  0.6 69.2 %shard_map.176 = (bf16[384,512]{1,0:T(8,128)(2,1)S(1)}, bf16[128,2048]{1,0:T(8,128)(2,1)S(1)}) custom-call(bf16[512,2048]{1,0:T(8,128)(2,1)} %xa_hbm.1, f32[2048]{0:T(1024)} %a_gain_hbm.1, bf16[2048,256]{1,0:T(8,128)(2,1)} %wq_hbm.1, bf16[2048,128]{1,0:T(8,128)(2,1)} %wk_hbm.1, bf16[2048,128]{1,0:T(8,128)(2,1)} %wv_hbm.1, f32[64]{0:T(128)} %q_gain_hbm.1, ...), custom_call_target="tpu_custom_call" | custom-call | tf_op jit(solution)/shard_map/pallas_call | solution.py:687
  69.9 0.8 %copy.21 = bf16[128,2048]{1,0:T(8,128)(2,1)} copy(bf16[128,2048]{1,0:T(8,128)(2,1)S(1)} %get-tuple-element.6) | data formatting | bytes 1048576
  70.7 0.7 %copy.22 = bf16[384,512]{1,0:T(8,128)(2,1)} copy(bf16[384,512]{1,0:T(8,128)(2,1)S(1)} %get-tuple-element.7) | data formatting | bytes 786432

commit v4 on v3

--- a/solution.py
+++ b/solution.py
@@ -250,7 +250,7 @@
         rows_buf[across, 0] = gathered(chosen, across)
         relay(0).start()
 
-    def build_mix():
+    def build_mix(part):
         columns = iota((moe_tokens, n_ep), 1)
         slots = iota((moe_tokens, capacity), 1).astype(f32)
 
@@ -260,7 +260,7 @@
             mix[e] = jnp.where(rank == slots, share, 0.0).astype(bf16)
             return carry
 
-        lax.fori_loop(0, n_ep, body, 0)
+        lax.fori_loop(part * (n_ep // 2), (part + 1) * (n_ep // 2), body, 0)
 
     def A(k, near):
         dispatch(k).wait_recv()
@@ -326,8 +326,8 @@
                     by_row, rows[r : r + 1, :], cols
                 )
 
-    def qkv():
-        step = min(256, tokens)
+    def qkv(first, last):
+        step = tokens // 2
         lanes = iota((1, pair), 1)
         low = lax.rem(lanes, HEAD_DIM) < HEAD_DIM // 2
         ones = one_zero(
@@ -365,7 +365,7 @@
             kv[rows, kw : 2 * kw] = x[:, q_cols + kw :].astype(bf16)
             return carry
 
-        lax.fori_loop(0, tokens // step, body, 0)
+        lax.fori_loop(first, last, body, 0)
 
     def expand(src, start, rows):
         block = jnp.concatenate([src[:, 0:kw], src[:, kw : 2 * kw]], axis=0)
@@ -441,7 +441,7 @@
 
         lax.fori_loop(0, count, body, 0)
 
-    def project():
+    def project(part):
         tile = 2 * pair
         quarter = attn_ref.shape[1]
 
@@ -452,9 +452,11 @@
                 attn_ref[s, :, cols] = x[s * quarter : (s + 1) * quarter]
             return carry
 
-        lax.fori_loop(0, wo.shape[1] // tile, body, 0)
-        attn_core(0).start()
-        attn_core(1).start()
+        count = wo.shape[1] // tile // 2
+        lax.fori_loop(part * count, (part + 1) * count, body, 0)
+        if part == 1:
+            attn_core(0).start()
+            attn_core(1).start()
 
     def attn_sum():
         attn_core(0).wait_recv()
@@ -500,93 +502,188 @@
         loads[3].wait()
         rms_inplace(xa, 0, tokens, a_gain)
 
-    def front_qkv():
-        for copy in loads[4:8]:
-            copy.wait()
-        rope_tables()
-        qkv()
+    def front_qkv(part):
+        if part == 0:
+            for copy in loads[4:8]:
+                copy.wait()
+            rope_tables()
+        qkv(part, part + 1)
 
     if n_ep == 8:
-        D(6, False)
-        L0()
-        D(1, True)
-        D(4, False)
-        front_norm()
-        D(2, True)
-        D(7, False)
-        load_ffn()
-        C(0)
-        front_qkv()
-        A(6, False)
-        build_mix()
-        E(0)
-        halo_start()
-        B(6)
-        A(4, False)
-        Z(1)
-        Z(2)
-        A(2, True)
-        C(6)
-        F(0, True)
-        E(6)
-        B(4)
-        D(5, False)
-        D(3, True)
-        C(2)
-        A(7, False)
-        A(1, True)
-        C(4)
-        E(2)
-        halo_finish()
-        expand(kv, WINDOW, tokens)
-        F(6, False)
-        E(4)
-        attend(0, 2, nb - 1)
-        attend(1, nb - 2, 1)
-        C(1)
-        B(7)
-        project()
-        A(5, False)
-        A(3, True)
-        C(7)
-        E(1)
-        E(7)
-        F(4, False)
-        B(5)
-        G(6)
-        attn_sum()
-        F(2, False)
-        Z(3)
-        C(5)
-        attn_cross(1)
-        C(3)
-        F(1, False)
-        attn_cross(6)
-        E(5)
-        F(7, False)
-        E(3)
-        attn_cross(0)
-        G(2)
-        attn_final(1)
-        attn_cross(2)
-        F(5, False)
-        attn_cross(4)
-        F(3, False)
-        attn_cross(3)
-        attn_cross(5)
-        attn_final(0)
-        G(4)
-        G(1)
-        attn_cross(7)
-        attn_final(5)
-        attn_final(6)
-        attn_final(4)
-        G(7)
-        attn_final(2)
-        G(5)
-        attn_final(3)
-        G(3)
-        attn_final(7)
+        inner = lax.rem(me // (n_ep // 4) + 1, 4) // 2
+
+        @pl.when(inner == 1)
+        def _():
+            D(5, False)
+            L0()
+            D(1, True)
+            D(2, True)
+            D(6, False)
+            load_ffn()
+            C(0)
+            front_norm()
+            front_qkv(0)
+            E(0)
+            D(3, True)
+            A(5, False)
+            B(5)
+            front_qkv(1)
+            D(7, False)
+            A(6, False)
+            C(5)
+            D(4, False)
+            expand(kv, WINDOW, tokens)
+            E(5)
+            halo_start()
+            A(4, False)
+            B(6)
+            A(3, True)
+            C(6)
+            Z(1)
+            A(7, False)
+            Z(3)
+            attend(1, nb - 2, 1)
+            A(2, True)
+            A(1, True)
+            build_mix(0)
+            E(6)
+            B(4)
+            C(3)
+            C(1)
+            B(7)
+            halo_finish()
+            E(3)
+            C(4)
+            E(1)
+            F(6, False)
+            attend(0, 2, nb - 1)
+            C(7)
+            F(5, False)
+            E(4)
+            project(0)
+            F(3, False)
+            Z(2)
+            build_mix(1)
+            project(1)
+            C(2)
+            E(7)
+            attn_sum()
+            F(1, False)
+            F(4, False)
+            attn_cross(6)
+            attn_cross(3)
+            E(2)
+            attn_cross(4)
+            attn_cross(7)
+            attn_cross(2)
+            F(7, False)
+            attn_final(6)
+            attn_cross(0)
+            attn_cross(1)
+            attn_final(4)
+            attn_final(3)
+            F(0, True)
+            G(3)
+            F(2, False)
+            G(2)
+            G(7)
+            G(1)
+            attn_cross(5)
+            attn_final(0)
+            attn_final(1)
+            G(5)
+            G(6)
+            attn_final(2)
+            attn_final(7)
+            attn_final(5)
+            G(4)
+
+        @pl.when(inner == 0)
+        def _():
+            D(5, False)
+            L0()
+            D(1, True)
+            front_norm()
+            load_ffn()
+            C(0)
+            D(6, False)
+            E(0)
+            front_qkv(0)
+            D(3, True)
+            front_qkv(1)
+            A(1, True)
+            A(6, False)
+            Z(1)
+            build_mix(0)
+            A(5, False)
+            D(4, False)
+            C(1)
+            E(1)
+            B(6)
+            build_mix(1)
+            D(2, True)
+            C(6)
+            B(5)
+            E(6)
+            expand(kv, WINDOW, tokens)
+            halo_start()
+            Z(2)
+            C(5)
+            D(7, False)
+            A(3, True)
+            Z(3)
+            E(5)
+            attend(1, nb - 2, 1)
+            C(3)
+            halo_finish()
+            A(2, True)
+            F(6, False)
+            A(4, False)
+            attend(0, 2, nb - 1)
+            project(0)
+            project(1)
+            E(3)
+            F(5, False)
+            B(4)
+            A(7, False)
+            C(2)
+            attn_sum()
+            attn_cross(6)
+            F(0, True)
+            attn_cross(3)
+            E(2)
+            F(3, False)
+            B(7)
+            attn_cross(4)
+            C(4)
+            C(7)
+            E(7)
+            F(1, False)
+            E(4)
+            F(2, False)
+            attn_cross(5)
+            F(7, False)
+            attn_cross(2)
+            attn_final(4)
+            G(5)
+            attn_cross(0)
+            F(4, False)
+            attn_final(3)
+            attn_cross(1)
+            attn_cross(7)
+            attn_final(1)
+            attn_final(5)
+            attn_final(2)
+            G(3)
+            attn_final(6)
+            attn_final(0)
+            G(7)
+            G(4)
+            G(1)
+            G(2)
+            G(6)
+            attn_final(7)
+
     else:
         def each(low, high, fn):
             def body(k, carry):
@@ -600,7 +697,8 @@
         L0()
         load_ffn()
         front_norm()
-        front_qkv()
+        front_qkv(0)
+        front_qkv(1)
         halo_start()
         expand(kv, WINDOW, tokens)
         attend(1, nb - 2, 1)
@@ -609,8 +707,10 @@
         each(half, n_ep, lambda k: A(k, False))
         halo_finish()
         attend(0, 2, nb - 1)
-        project()
-        build_mix()
+        project(0)
+        project(1)
+        build_mix(0)
+        build_mix(1)
         each(half, n_ep, B)
         each(0, n_ep, C)
         each(0, n_ep, E)

time: 71.6 us -> 68 us (0.950)
  Pallas kernels: 69.2 us -> 65.6 us
    pallas_call x1, Pallas kernels: 69.2 us -> 65.6 us  [per_device(): pl.pallas_call(functools.partial(fused_kernel, n_ep), out_shape=(buf(moe_...]
where the time goes in v4:
time: 68 us; the launch traced here: 67.8 us
  Pallas kernels  65.6 us (96%)
  local copies, waits for them, and re-layouts  1.54 us (2%)
    pallas_call x1, Pallas kernels, per_device(): pl.pallas_call(functools.partial(fused_kernel, n_ep), out_shape=(buf(moe_...  65.6 us
    unnamed x2, local copies, waits for them, and re-layouts  1.54 us

profile of v4, /device:TPU:0, one launch (start us, length us, event | category | flops | bytes accessed | tf_op | source)
XLA Modules:
  0.0 67.8 jit_solution(10404529765482121926)
XLA Ops:
  0.6 65.6 %shard_map.176 = (bf16[384,512]{1,0:T(8,128)(2,1)S(1)}, bf16[128,2048]{1,0:T(8,128)(2,1)S(1)}) custom-call(bf16[512,2048]{1,0:T(8,128)(2,1)} %xa_hbm.1, f32[2048]{0:T(1024)} %a_gain_hbm.1, bf16[2048,256]{1,0:T(8,128)(2,1)} %wq_hbm.1, bf16[2048,128]{1,0:T(8,128)(2,1)} %wk_hbm.1, bf16[2048,128]{1,0:T(8,128)(2,1)} %wv_hbm.1, f32[64]{0:T(128)} %q_gain_hbm.1, ...), custom_call_target="tpu_custom_call" | custom-call | tf_op jit(solution)/shard_map/pallas_call | solution.py:787
  66.3 0.8 %copy.21 = bf16[128,2048]{1,0:T(8,128)(2,1)} copy(bf16[128,2048]{1,0:T(8,128)(2,1)S(1)} %get-tuple-element.6) | data formatting | bytes 1048576
  67.1 0.7 %copy.22 = bf16[384,512]{1,0:T(8,128)(2,1)} copy(bf16[384,512]{1,0:T(8,128)(2,1)S(1)} %get-tuple-element.7) | data formatting | bytes 786432

commit v5 on v4

--- a/solution.py
+++ b/solution.py
@@ -124,6 +124,18 @@
             ]
         )
     ]
+    barrier = pltpu.get_barrier_semaphore()
+
+    def greet(k, carry):
+        pl.semaphore_signal(
+            barrier, inc=1, device_id={"ep": flip(me, k, n_ep), "tp": lane}, device_id_type=MESH
+        )
+        return carry
+
+    lax.fori_loop(1, n_ep, greet, 0)
+    for peer in (partner, across):
+        pl.semaphore_signal(barrier, inc=1, device_id={"ep": me, "tp": peer}, device_id_type=MESH)
+
     for copy in small:
         copy.start()
     first_rows = moe_tokens // XE_PIECES
@@ -137,18 +149,6 @@
     ]
     for copy in pieces:
         copy.start()
-
-    barrier = pltpu.get_barrier_semaphore()
-
-    def greet(k, carry):
-        pl.semaphore_signal(
-            barrier, inc=1, device_id={"ep": flip(me, k, n_ep), "tp": lane}, device_id_type=MESH
-        )
-        return carry
-
-    lax.fori_loop(1, n_ep, greet, 0)
-    for peer in (partner, across):
-        pl.semaphore_signal(barrier, inc=1, device_id={"ep": me, "tp": peer}, device_id_type=MESH)
 
     def remote(src, dst, sends, recvs, k, ep, tp):
         return pltpu.make_async_remote_copy(

time: 68 us -> 68.1 us (level)
  no operation moved by 1% of the time
where the time goes in v5:
time: 68.1 us; the launch traced here: 68 us
  Pallas kernels  65.8 us (97%)
  local copies, waits for them, and re-layouts  1.54 us (2%)
    pallas_call x1, Pallas kernels, per_device(): pl.pallas_call(functools.partial(fused_kernel, n_ep), out_shape=(buf(moe_...  65.8 us
    unnamed x2, local copies, waits for them, and re-layouts  1.54 us

profile of v5, /device:TPU:0, one launch (start us, length us, event | category | flops | bytes accessed | tf_op | source)
XLA Modules:
  0.0 68.0 jit_solution(3003414487331368564)
XLA Ops:
  0.6 65.8 %shard_map.176 = (bf16[384,512]{1,0:T(8,128)(2,1)S(1)}, bf16[128,2048]{1,0:T(8,128)(2,1)S(1)}) custom-call(bf16[512,2048]{1,0:T(8,128)(2,1)} %xa_hbm.1, f32[2048]{0:T(1024)} %a_gain_hbm.1, bf16[2048,256]{1,0:T(8,128)(2,1)} %wq_hbm.1, bf16[2048,128]{1,0:T(8,128)(2,1)} %wk_hbm.1, bf16[2048,128]{1,0:T(8,128)(2,1)} %wv_hbm.1, f32[64]{0:T(128)} %q_gain_hbm.1, ...), custom_call_target="tpu_custom_call" | custom-call | tf_op jit(solution)/shard_map/pallas_call | solution.py:787
  66.4 0.8 %copy.21 = bf16[128,2048]{1,0:T(8,128)(2,1)} copy(bf16[128,2048]{1,0:T(8,128)(2,1)S(1)} %get-tuple-element.6) | data formatting | bytes 1048576
  67.2 0.7 %copy.22 = bf16[384,512]{1,0:T(8,128)(2,1)} copy(bf16[384,512]{1,0:T(8,128)(2,1)S(1)} %get-tuple-element.7) | data formatting | bytes 786432
